TPU v7x, 32 devices: a whole 2x2x4 slice. The times are simulated.
32 devices in a mesh: sp: 16 (over z, y, x), tp: 2 (over core).
Axes of the slice: x: 2, y: 2, z: 4, core: 2. Of those that a mesh axis runs over, the one named last changes fastest.
Arguments:
- moe_input: bfloat16 [4096, 2048], P('sp'), may hold values from -6 to 6
- cotangent: bfloat16 [4096, 2048], P('sp'), may hold values from -6 to 6
- expert_ids: int32 [4096, 2], P('sp'), may hold values from 0 to 15, all different within a row; in each aligned block of 256 rows (0 to 255, 256 to 511, ...) at most 64 rows name the same one
- route_weight: float32 [4096, 2], P('sp'), may hold values from 0.05 to 0.6
- gate_proj: bfloat16 [16, 2048, 1024], P('sp', None, 'tp'), may hold values from -0.125 to 0.125
- up_proj: bfloat16 [16, 2048, 1024], P('sp', None, 'tp'), may hold values from -0.125 to 0.125
- down_proj: bfloat16 [16, 1024, 2048], P('sp', 'tp'), may hold values from -0.1875 to 0.1875
- out_weight: bfloat16 [2048, 2048], P(None, 'tp'), may hold values from -0.125 to 0.125
- recur_input: bfloat16 [4096, 2048], P('sp', 'tp'), may hold values from -6 to 6
- gate_input: bfloat16 [4096, 2048], P('sp', 'tp'), may hold values from -6 to 6
- states: float32 [4096, 2048], P('sp', 'tp'), may hold values from -6 to 6
- conv_taps: bfloat16 [4, 2048], P(None, 'tp'), may hold values from -3 to 3
- decay_gate_w: bfloat16 [16, 128, 128], P('tp'), may hold values from -0.5 to 0.5
- input_gate_w: bfloat16 [16, 128, 128], P('tp'), may hold values from -0.5 to 0.5
- decay_rate: float32 [2048], P('tp'), may hold values from 7.3242187e-06 to 0.008
- decay_extra: float32 [4096, 2048], P('sp', 'tp'), may hold values from -0.77 to 0
Outputs:
- gate_proj_grad: bfloat16 [16, 2048, 1024], P('sp', None, 'tp')
- up_proj_grad: bfloat16 [16, 2048, 1024], P('sp', None, 'tp')
- down_proj_grad: bfloat16 [16, 1024, 2048], P('sp', 'tp')
- out_weight_grad: float32 [2048, 2048], P('sp', 'tp')
- input_grad: bfloat16 [4096, 2048], P('sp')
- recur_grad: bfloat16 [4096, 2048], P('sp', 'tp')
- gate_grad: bfloat16 [4096, 2048], P('sp', 'tp')
Inputs may be any that keep to these rules, and one draw needn't show every extreme that they name: `expert_ids`: within each aligned block of 256 tokens a token names 2 different experts, and no expert is named more than 64 times.
All inputs are finite; a program needn't handle non-finite values.
Results may differ from a plain program's by a relative error of at most 0.012.
Values may be sent and summed in bfloat16 or wider, within the bound.
A program may use at most 128 MiB of HBM per device.

v0:
```python
import jax
import jax.numpy as jnp
from jax import lax
from jax.experimental import pallas as pl
from jax.experimental.pallas import tpu as pltpu
from jax.sharding import PartitionSpec as P

decay_scale = 8.0


def passed_along(value, axis, steps):
    count = lax.axis_size(axis)
    initial, last = (max(0, -steps), min(count, count - steps))
    return lax.ppermute(value, axis, [(source, source + steps) for source in range(initial, last)])


def swapped(value, axis):
    return lax.ppermute(value, axis, [(0, 1), (1, 0)])


def carried_in(product, total, axis):
    count, mine = (lax.axis_size(axis), lax.axis_index(axis))
    pair = jnp.stack([product, total])
    pieces = lax.all_to_all(
        jnp.broadcast_to(pair[None], (count,) + pair.shape),
        axis,
        split_axis=0,
        concat_axis=0,
        tiled=True,
    )
    entering = jnp.zeros_like(total)
    for position in range(count - 1, 0, -1):
        longer = pieces[position, 0] * entering + pieces[position, 1]
        entering = jnp.where(position > mine, longer, entering)
    return entering


def scan_kernel(decay_ref, grad_ref, product_ref, local_ref):
    rows, lanes = decay_ref.shape
    group = 8
    last = rows // group - 1

    def step(index, carry):
        product, total, decay = carry
        start = pl.multiple_of((last - index) * group, group)
        decays = decay_ref[pl.ds(start, group), :]
        grads = grad_ref[pl.ds(start, group), :]
        products, totals = ([None] * group, [None] * group)
        for row in range(group - 1, -1, -1):
            product = product * decay
            total = grads[row : row + 1] + decay * total
            decay = decays[row : row + 1]
            products[row], totals[row] = (product, total)
        product_ref[pl.ds(start, group), :] = jnp.concatenate(products, axis=0)
        local_ref[pl.ds(start, group), :] = jnp.concatenate(totals, axis=0)
        return (product, total, decay)

    one = jnp.ones((1, lanes), jnp.float32)
    lax.fori_loop(0, last + 1, step, (one, jnp.zeros_like(one), one))


def reverse_scan(decay, grad):
    rows, channels = decay.shape
    width = 512 if channels % 512 == 0 else channels
    block = pl.BlockSpec((rows, width), lambda index: (0, index))
    return pl.pallas_call(
        scan_kernel,
        grid=(channels // width,),
        in_specs=[block, block],
        out_specs=[block, block],
        out_shape=[jax.ShapeDtypeStruct(decay.shape, jnp.float32)] * 2,
        cost_estimate=pl.CostEstimate(
            flops=3 * rows * channels, bytes_accessed=16 * rows * channels, transcendentals=0
        ),
        name="reverse_scan",
    )(decay, grad)


def contract_rows(left, right):
    return lax.dot_general(
        left, right, (((0,), (0,)), ((), ())), preferred_element_type=jnp.float32
    )


def contract_cols(left, right):
    return lax.dot_general(
        left, right, (((1,), (1,)), ((), ())), preferred_element_type=jnp.float32
    )


def on_device(
    moe_input,
    cotangent,
    expert_ids,
    route_weight,
    gate_proj,
    up_proj,
    down_proj,
    out_weight,
    recur_input,
    gate_input,
    states,
    conv_taps,
    decay_gate_w,
    input_gate_w,
    decay_rate,
    decay_extra,
):
    experts = lax.axis_size("sp")
    cores = lax.axis_size("tp")
    tok_rows, width = moe_input.shape
    top_count = expert_ids.shape[1]
    capacity = max(2, 4 * tok_rows // experts)
    slot_count = experts * capacity
    gate_float = gate_input.astype(jnp.float32)
    gelu_value, gelu_back = jax.vjp(jax.nn.gelu, gate_float)
    mixer_out = (states * gelu_value).astype(jnp.bfloat16)
    mixer_all = lax.all_gather(mixer_out, "sp", axis=0, tiled=True)
    flat_ids = expert_ids.reshape(-1)
    onehot = (flat_ids[:, None] == jnp.arange(experts, dtype=jnp.int32)[None, :]).astype(jnp.int32)
    slot_rank = jnp.sum((jnp.cumsum(onehot, axis=0) - onehot) * onehot, axis=1)
    target = flat_ids * capacity + slot_rank
    slot_iota = jnp.arange(slot_count, dtype=jnp.int32)
    placing = (slot_iota[:, None] == target[None, :]).astype(jnp.bfloat16)
    pair_slots = target.reshape(tok_rows, top_count)
    placing_tok = jnp.any(slot_iota[:, None, None] == pair_slots[None, :, :], axis=2).astype(
        jnp.bfloat16
    )
    scaled = (route_weight[:, :, None] * cotangent.astype(jnp.float32)[:, None, :]).astype(
        jnp.bfloat16
    )
    scaled = scaled.reshape(tok_rows * top_count, width)
    send_rows = jnp.dot(placing_tok, moe_input, preferred_element_type=jnp.float32).astype(
        jnp.bfloat16
    )
    send_rows = send_rows.reshape(experts, capacity, width)
    send_grads = jnp.dot(placing, scaled, preferred_element_type=jnp.float32).astype(jnp.bfloat16)
    send_grads = send_grads.reshape(experts, capacity, width)
    share_size = capacity // cores
    offset = lax.axis_index("tp") * share_size
    mine_rows = lax.dynamic_slice_in_dim(send_rows, offset, share_size, 1)
    mine_grads = lax.dynamic_slice_in_dim(send_grads, offset, share_size, 1)
    got_rows = lax.all_to_all(mine_rows, "sp", split_axis=0, concat_axis=0, tiled=True)
    got_grads = lax.all_to_all(mine_grads, "sp", split_axis=0, concat_axis=0, tiled=True)
    got_rows = got_rows.reshape(experts * share_size, width)
    got_grads = got_grads.reshape(experts * share_size, width)
    rows_in = jnp.concatenate([got_rows, swapped(got_rows, "tp")], axis=0)
    grads_in = jnp.concatenate([got_grads, swapped(got_grads, "tp")], axis=0)
    weight_gate = gate_proj[0]
    weight_up = up_proj[0]
    weight_down = down_proj[0]
    gate_pre = jnp.dot(rows_in, weight_gate, preferred_element_type=jnp.float32)
    up_pre = jnp.dot(rows_in, weight_up, preferred_element_type=jnp.float32)
    sigmoid_gate = jax.nn.sigmoid(gate_pre)
    silu_gate = gate_pre * sigmoid_gate
    hidden = (silu_gate * up_pre).astype(jnp.bfloat16)
    down_grad = contract_rows(hidden, grads_in)
    hidden_grad = contract_cols(grads_in, weight_down)
    gate_pre_grad = (
        hidden_grad * up_pre * sigmoid_gate * (1.0 + gate_pre * (1.0 - sigmoid_gate))
    ).astype(jnp.bfloat16)
    up_pre_grad = (hidden_grad * silu_gate).astype(jnp.bfloat16)
    gate_weight_grad = contract_rows(rows_in, gate_pre_grad)
    up_weight_grad = contract_rows(rows_in, up_pre_grad)
    half = experts * share_size
    other_part = (
        contract_cols(gate_pre_grad[half:], weight_gate)
        + contract_cols(up_pre_grad[half:], weight_up)
    ).astype(jnp.bfloat16)
    arrived_part = swapped(other_part, "tp").astype(jnp.float32)
    own_part = contract_cols(gate_pre_grad[:half], weight_gate) + contract_cols(
        up_pre_grad[:half], weight_up
    )
    shared = (own_part + arrived_part).astype(jnp.bfloat16)
    shared, mixer_all = lax.optimization_barrier((shared, mixer_all))
    back_half = lax.all_to_all(
        shared.reshape(experts, share_size, width), "sp", split_axis=0, concat_axis=0, tiled=True
    )
    placing_half = lax.dynamic_slice_in_dim(
        placing_tok.reshape(experts, capacity, tok_rows), offset, share_size, 1
    ).reshape(half, tok_rows)
    moe_part = contract_rows(placing_half, back_half.reshape(half, width)).astype(jnp.bfloat16)
    moe_grad = moe_part.astype(jnp.float32) + swapped(moe_part, "tp").astype(jnp.float32)
    input_grad = (moe_grad + cotangent.astype(jnp.float32)).astype(jnp.bfloat16)
    column_share = width // experts
    grad_columns = lax.all_to_all(
        input_grad.reshape(tok_rows, experts, column_share).transpose(1, 0, 2),
        "sp",
        split_axis=0,
        concat_axis=0,
        tiled=True,
    ).reshape(experts * tok_rows, column_share)
    out_weight_grad = contract_rows(grad_columns, mixer_all)
    mixer_grad = jnp.dot(input_grad, out_weight, preferred_element_type=jnp.float32)
    gate_grad = gelu_back(mixer_grad * states)[0].astype(jnp.bfloat16)
    state_grad = mixer_grad * gelu_value
    channels = recur_input.shape[1]
    prev_inputs, prev_state = passed_along(
        (recur_input[-3:].astype(jnp.float32), states[-1:]), "sp", 1
    )
    extended = jnp.concatenate([prev_inputs, recur_input.astype(jnp.float32)], axis=0)
    taps = conv_taps.astype(jnp.float32)
    conv = taps[0] * extended[0:tok_rows]
    for tap_index in range(1, 4):
        conv = conv + taps[tap_index] * extended[tap_index : tap_index + tok_rows]
    blocks = decay_gate_w.shape[0]
    block_width = decay_gate_w.shape[1]
    conv_blocks = conv.astype(jnp.bfloat16).reshape(tok_rows, blocks, block_width)
    decay_pre = jnp.einsum(
        "tbi,bij->tbj", conv_blocks, decay_gate_w, preferred_element_type=jnp.float32
    ).reshape(tok_rows, channels)
    input_pre = jnp.einsum(
        "tbi,bij->tbj", conv_blocks, input_gate_w, preferred_element_type=jnp.float32
    ).reshape(tok_rows, channels)
    recur_gate = jax.nn.sigmoid(decay_pre)
    input_gate = jax.nn.sigmoid(input_pre)
    positions = lax.axis_index("sp") * tok_rows + jnp.arange(tok_rows, dtype=jnp.int32)
    first_row = (positions == 0)[:, None]
    log_decay = -decay_scale * recur_gate * decay_rate[None, :] + decay_extra
    decay_value = jnp.exp(log_decay)
    mult = jnp.where(first_row, 1.0, jnp.sqrt(-jnp.expm1(2.0 * log_decay)))
    prev_states = jnp.concatenate([prev_state, states[:-1]], axis=0)
    cumul, local_values = reverse_scan(decay_value, state_grad)
    entering = carried_in(decay_value[0] * cumul[0], decay_value[0] * local_values[0], "sp")
    carried_grad = local_values + cumul * entering[None, :]
    log_grad = carried_grad * prev_states * decay_value - jnp.where(
        first_row, 0.0, carried_grad * input_gate * conv * decay_value * decay_value / mult
    )
    decay_pre_grad = (
        log_grad * (-decay_scale * decay_rate[None, :]) * recur_gate * (1.0 - recur_gate)
    ).astype(jnp.bfloat16)
    input_pre_grad = (carried_grad * mult * conv * input_gate * (1.0 - input_gate)).astype(
        jnp.bfloat16
    )
    conv_grad = (
        carried_grad * mult * input_gate
        + jnp.einsum(
            "tbj,bij->tbi",
            decay_pre_grad.reshape(tok_rows, blocks, block_width),
            decay_gate_w,
            preferred_element_type=jnp.float32,
        ).reshape(tok_rows, channels)
        + jnp.einsum(
            "tbj,bij->tbi",
            input_pre_grad.reshape(tok_rows, blocks, block_width),
            input_gate_w,
            preferred_element_type=jnp.float32,
        ).reshape(tok_rows, channels)
    )
    next_grads = passed_along(conv_grad[:3], "sp", -1)
    grad_extended = jnp.concatenate([conv_grad, next_grads], axis=0)
    recur_float = taps[0] * grad_extended[3 : 3 + tok_rows]
    for tap_index in range(1, 4):
        recur_float = (
            recur_float + taps[tap_index] * grad_extended[3 - tap_index : 3 - tap_index + tok_rows]
        )
    recur_grad = recur_float.astype(jnp.bfloat16)
    return (
        gate_weight_grad.astype(jnp.bfloat16)[None],
        up_weight_grad.astype(jnp.bfloat16)[None],
        down_grad.astype(jnp.bfloat16)[None],
        out_weight_grad,
        input_grad,
        recur_grad,
        gate_grad,
    )


def solution(mesh):
    return jax.shard_map(
        on_device,
        mesh=mesh,
        in_specs=(
            P("sp", None),
            P("sp", None),
            P("sp", None),
            P("sp", None),
            P("sp", None, "tp"),
            P("sp", None, "tp"),
            P("sp", "tp", None),
            P(None, "tp"),
            P("sp", "tp"),
            P("sp", "tp"),
            P("sp", "tp"),
            P(None, "tp"),
            P("tp", None, None),
            P("tp", None, None),
            P("tp"),
            P("sp", "tp"),
        ),
        out_specs=(
            P("sp", None, "tp"),
            P("sp", None, "tp"),
            P("sp", "tp", None),
            P("sp", "tp"),
            P("sp", None),
            P("sp", "tp"),
            P("sp", "tp"),
        ),
        check_vma=False,
    )
```

profile of v0, /device:TPU:14, one launch (start us, length us, event | category | flops | bytes accessed | tf_op | source)
XLA Modules:
  0.0 371.6 jit_solution(6248571824596983457)
XLA Ops:
  7.2 2.7 multiply_convert_fusion.7
  10.0 0.1 copy.69
  10.1 0.1 eq.62
  10.2 0.1 eq.66
  10.4 1.2 reduce-window.6
  11.6 0.2 slice_reduce_fusion
  11.9 0.1 reduce_sum.12
  12.2 0.4 fusion.18
  12.6 2.5 convolution_convert_fusion.1
  15.0 1.6 constant_dynamic-slice_fusion.1
  16.6 7.3 %all-to-all-start = ((bf16[16,32,2048]{2,1,0:T(8,128)(2,1)}), bf16[16,32,2048]{2,1,0:T(8,128)(2,1)}, u32[]{:S(2)}, u32[]{:S(2)}) async-start(bf16[16,32,2048]{2,1,0:T(8,128)(2,1)} %constant_dynamic-slice_fusion.1), calls=%async_computation | async-start | bytes 4194304 | tf_op jit(solution)/shard_map/all_to_all | solution.py:143
  23.9 4.2 %mul.380 = f32[256,2,2048]{2,1,0:T(2,128)} broadcast(bf16[256,2048]{1,0:T(8,128)(2,1)S(1)} %copy-done.4), dimensions={0,2} | broadcast | bytes 5242880 | tf_op jit(solution)/shard_map/mul | solution.py:129
  28.1 6.1 %mul.381 = f32[512,2048]{1,0:T(8,128)} reshape(f32[256,2,2048]{2,1,0:T(2,128)} %mul.380) | data formatting | bytes 8388608 | tf_op jit(solution)/shard_map/mul | solution.py:129
  34.1 0.1 copy.73
  34.3 0.1 mul.378
  34.4 4.6 %convolution_convert_fusion = bf16[1024,2048]{1,0:T(8,128)(2,1)S(1)} fusion(f32[512,2048]{1,0:T(8,128)} %mul.381, f32[512]{0:T(512)S(1)} %mul.378, s32[512]{0:T(512)S(1)} %multiply_add_fusion.2), kind=kOutput, calls=%fused_computation.5 | convolution fusion | flops 2152202240 | bytes 8392704 | tf_op jit(solution)/shard_map/dot_general | solution.py:137
  39.1 1.6 constant_dynamic-slice_fusion
  40.6 62.5 %all-to-all-done = bf16[16,32,2048]{2,1,0:T(8,128)(2,1)} async-done(((bf16[16,32,2048]{2,1,0:T(8,128)(2,1)}), bf16[16,32,2048]{2,1,0:T(8,128)(2,1)}, u32[]{:S(2)}, u32[]{:S(2)}) %all-to-all-start) | async-done | bytes 2097184 | tf_op jit(solution)/shard_map/all_to_all | solution.py:143
  103.1 6.0 %all-to-all-start.1 = ((bf16[16,32,2048]{2,1,0:T(8,128)(2,1)}), bf16[16,32,2048]{2,1,0:T(8,128)(2,1)}, u32[]{:S(2)}, u32[]{:S(2)}) async-start(bf16[16,32,2048]{2,1,0:T(8,128)(2,1)} %constant_dynamic-slice_fusion), calls=%async_computation.1 | async-start | bytes 4194304 | tf_op jit(solution)/shard_map/all_to_all | solution.py:144
  109.2 91.7 %all-to-all-done.1 = bf16[16,32,2048]{2,1,0:T(8,128)(2,1)} async-done(((bf16[16,32,2048]{2,1,0:T(8,128)(2,1)}), bf16[16,32,2048]{2,1,0:T(8,128)(2,1)}, u32[]{:S(2)}, u32[]{:S(2)}) %all-to-all-start.1) | async-done | bytes 2097184 | tf_op jit(solution)/shard_map/all_to_all | solution.py:144
  201.0 4.7 %fusion.9 = f32[1024,512]{1,0:T(8,128)S(1)} fusion(bf16[1,2048,512]{2,1,0:T(8,128)(2,1)S(1)} %copy-done, bf16[512,2048]{1,0:T(8,128)(2,1)} %collective-permute-done, bf16[512,2048]{1,0:T(8,128)(2,1)} %bitcast.2), kind=kOutput, calls=%fused_computation.20 | convolution fusion | flops 2155872256 | bytes 8388608 | tf_op jit(solution)/shard_map/dot_general | solution.py:152
  205.7 5.4 %fusion.13 = f32[1024,512]{1,0:T(8,128)S(1)} fusion(bf16[1,2048,512]{2,1,0:T(8,128)(2,1)S(1)} %copy-done.2, bf16[512,2048]{1,0:T(8,128)(2,1)} %collective-permute-done, bf16[512,2048]{1,0:T(8,128)(2,1)} %bitcast.2), kind=kOutput, calls=%fused_computation.24 | convolution fusion | flops 2155872256 | bytes 8388608 | tf_op jit(solution)/shard_map/dot_general | solution.py:153
  211.1 6.1 %multiply_convert_fusion.3 = (bf16[1024,512]{1,0:T(8,128)(2,1)S(1)}, bf16[1024,512]{1,0:T(8,128)(2,1)S(1)}) fusion(f32[1024,512]{1,0:T(8,128)S(1)} %fusion.9, f32[1024,512]{1,0:T(8,128)S(1)} %fusion.13, bf16[1,512,2048]{2,1,0:T(8,128)(2,1)S(1)} %copy-done.22, bf16[512,2048]{1,0:T(8,128)(2,1)S(1)} %collective-permute-done.1, bf16[512,2048]{1,0:T(8,128)(2,1)} %bitcast.4), kind=kOutput, calls=%fused_computation.34 | convolution fusion | flops 2162688000 | bytes 12582912 | tf_op jit(solution)/shard_map/dot_general | solution.py:86
  217.3 1.3 fusion.5
  218.6 1.3 add_convert_fusion.1
  219.9 0.4 collective-permute-start.2
  220.3 1.3 fusion.7
  221.6 2.5 collective-permute-done.2
  224.1 2.7 add_convert_fusion
  226.8 5.3 %all-to-all-start.2 = ((bf16[16,32,2048]{2,1,0:T(8,128)(2,1)}), bf16[16,32,2048]{2,1,0:T(8,128)(2,1)}, u32[]{:S(2)}, u32[]{:S(2)}) async-start(bf16[16,32,2048]{2,1,0:T(8,128)(2,1)} %bitcast.12), calls=%async_computation.2 | async-start | bytes 4194304 | tf_op jit(solution)/shard_map/all_to_all | solution.py:176
  232.1 3.4 collective-permute-start.4
  235.5 3.6 collective-permute-start.5
  239.2 0.1 convert_element_type.115
  239.3 39.6 %collective-permute-done.4 = f32[3,1024]{1,0:T(4,128)S(1)} collective-permute-done((f32[3,1024]{1,0:T(4,128)S(1)}, f32[3,1024]{1,0:T(4,128)S(1)}, u32[]{:S(2)}, u32[]{:S(2)}) %collective-permute-start.4) | collective-permute-done | bytes 12320 | tf_op jit(solution)/shard_map/ppermute | solution.py:14
  278.9 1.5 convert_bitcast_fusion
  280.4 1.6 fusion.22
  282.0 0.3 copy.88
  282.4 2.6 fusion.25
  285.0 1.6 copy.87
  286.5 2.5 fusion.80.decay_ref
  289.0 2.4 fusion.4
  291.6 6.1 %fusion = bf16[1,2048,512]{2,1,0:T(8,128)(2,1)} fusion(bf16[1024,512]{1,0:T(8,128)(2,1)S(1)} %copy-done.9, bf16[512,2048]{1,0:T(8,128)(2,1)} %collective-permute-done, bf16[512,2048]{1,0:T(8,128)(2,1)} %bitcast.2), kind=kOutput, calls=%fused_computation.11 | convolution fusion | flops 2156920832 | bytes 7340032 | tf_op jit(solution)/shard_map/dot_general | solution.py:80
  297.7 5.7 %fusion.2 = bf16[1,512,2048]{2,1,0:T(8,128)(2,1)} fusion(bf16[512,2048]{1,0:T(8,128)(2,1)S(1)} %copy-done.24, bf16[512,2048]{1,0:T(8,128)(2,1)} %bitcast.4, f32[1024,512]{1,0:T(8,128)S(1)} %copy-done.28, f32[1024,512]{1,0:T(8,128)S(1)} %copy-done.26), kind=kOutput, calls=%fused_computation.13 | convolution fusion | flops 2160066560 | bytes 10485760 | tf_op jit(solution)/shard_map/dot_general | solution.py:80
  303.4 0.5 add_convert_fusion.2
  304.0 0.5 copy-done.13
  304.5 3.1 fusion.28
  307.6 5.3 %reverse_scan.1 = (f32[256,1024]{1,0:T(8,128)}, f32[256,1024]{1,0:T(8,128)}) custom-call(f32[256,1024]{1,0:T(8,128)} %fusion.80.decay_ref, f32[256,1024]{1,0:T(8,128)} %get-tuple-element.23.grad_ref), custom_call_target="tpu_custom_call" | custom-call | flops 786432 | bytes 4194304 | tf_op jit(solution)/shard_map/reverse_scan/pallas_call | solution.py:66
  312.9 0.8 slice_multiply_fusion.2
  313.7 0.7 broadcast_in_dim.47
  314.4 7.0 %all-to-all-start.4 = ((f32[16,2,1024]{2,1,0:T(2,128)}), f32[16,2,1024]{2,1,0:T(2,128)S(1)}, u32[]{:S(2)}, u32[]{:S(2)}) async-start(f32[16,2,1024]{2,1,0:T(2,128)} %broadcast_in_dim.47), calls=%async_computation.4 | async-start | bytes 262144 | tf_op jit(solution)/shard_map/all_to_all | solution.py:24
  321.4 1.2 bitcast_bitcast_fusion
  322.6 4.1 %all-to-all-done.4 = f32[16,2,1024]{2,1,0:T(2,128)S(1)} async-done(((f32[16,2,1024]{2,1,0:T(2,128)}), f32[16,2,1024]{2,1,0:T(2,128)S(1)}, u32[]{:S(2)}, u32[]{:S(2)}) %all-to-all-start.4) | async-done | bytes 131104 | tf_op jit(solution)/shard_map/all_to_all | solution.py:24
  326.7 6.7 %all-to-all-start.3 = ((bf16[16,256,128]{2,1,0:T(8,128)(2,1)}), bf16[16,256,128]{2,1,0:T(8,128)(2,1)S(1)}, u32[]{:S(2)}, u32[]{:S(2)}) async-start(bf16[16,256,128]{2,1,0:T(8,128)(2,1)} %bitcast_bitcast_fusion), calls=%async_computation.3 | async-start | bytes 2097152 | tf_op jit(solution)/shard_map/all_to_all | solution.py:186
  333.6 5.4 %fusion.62 = (bf16[32,8,8,128]{3,2,1,0:T(8,128)(2,1)S(1)}, f32[256,1024]{1,0:T(8,128)}, bf16[32,8,8,128]{3,2,1,0:T(8,128)(2,1)}) fusion(f32[256,1024]{1,0:T(8,128)S(1)} %copy.88, f32[256,1024]{1,0:T(8,128)} %get-tuple-element.18, f32[256,1024]{1,0:T(8,128)} %param.31, f32[256,1024]{1,0:T(8,128)S(1)} %copy.87, f32[1024]{0:T(1024)S(1)} %broadcast_multiply_fusion, ...), kind=kLoop, calls=%fused_computation.102 | loop fusion | flops 7340032 | bytes 9445632
  339.0 0.3 fusion.63
  339.3 1.3 copy.90
  340.6 1.3 fusion.66
  341.9 1.3 copy.89
  343.3 2.4 add_add_fusion
  345.7 2.5 collective-permute-start.6
  348.2 5.9 %fusion.1 = bf16[1,2048,512]{2,1,0:T(8,128)(2,1)} fusion(bf16[1024,512]{1,0:T(8,128)(2,1)S(1)} %copy-done.11, bf16[512,2048]{1,0:T(8,128)(2,1)} %collective-permute-done, bf16[512,2048]{1,0:T(8,128)(2,1)} %bitcast.2), kind=kOutput, calls=%fused_computation.12 | convolution fusion | flops 2156920832 | bytes 7340032 | tf_op jit(solution)/shard_map/dot_general | solution.py:80
  354.1 3.3 collective-permute-done.6
  357.4 1.3 fusion.34
  358.7 5.6 %fusion.94 = f32[128,1024]{1,0:T(8,128)} fusion(bf16[4096,128]{1,0:T(8,128)(2,1)S(1)} %bitcast.139, bf16[4096,1024]{1,0:T(8,128)(2,1)} %all-gather.2.cloned.1.call-done), kind=kOutput, calls=%fused_computation.151 | convolution fusion | flops 1073741824 | bytes 9961472 | tf_op jit(solution)/shard_map/dot_general | solution.py:80
  (86 shorter events, 0.8 us)
Async XLA Ops:
  7.2 193.8 %copy-start = (bf16[1,2048,512]{2,1,0:T(8,128)(2,1)S(1)}, bf16[1,2048,512]{2,1,0:T(8,128)(2,1)}, u32[]{:S(2)}) copy-start(bf16[1,2048,512]{2,1,0:T(8,128)(2,1)} %param.20) | copy-start | bytes 6291460
  7.2 2.8 copy-start.18
  7.2 219.6 %all-gather.2.cloned.1.call-start = ((), (), s32[]{:S(2)}) async-start(), calls=%async_computation.5 | async-start | bytes 8912896 | tf_op jit(solution)/shard_map/all_gather | solution.py:118
  16.6 7.3 %copy-start.4 = (bf16[256,2048]{1,0:T(8,128)(2,1)S(1)}, bf16[256,2048]{1,0:T(8,128)(2,1)}, u32[]{:S(2)}) copy-start(bf16[256,2048]{1,0:T(8,128)(2,1)} %param.17) | copy-start | bytes 3145732
  16.6 86.5 %all-to-all-start = ((bf16[16,32,2048]{2,1,0:T(8,128)(2,1)}), bf16[16,32,2048]{2,1,0:T(8,128)(2,1)}, u32[]{:S(2)}, u32[]{:S(2)}) async-start(bf16[16,32,2048]{2,1,0:T(8,128)(2,1)} %constant_dynamic-slice_fusion.1), calls=%async_computation | async-start | bytes 4194304 | tf_op jit(solution)/shard_map/all_to_all | solution.py:143
  28.1 6.1 %copy-start.20 = (f32[256,2]{0,1:T(2,128)S(1)}, f32[256,2]{0,1:T(2,128)}, u32[]{:S(2)}) copy-start(f32[256,2]{0,1:T(2,128)} %param.19) | copy-start | bytes 6148
  103.1 97.9 %all-to-all-start.1 = ((bf16[16,32,2048]{2,1,0:T(8,128)(2,1)}), bf16[16,32,2048]{2,1,0:T(8,128)(2,1)}, u32[]{:S(2)}, u32[]{:S(2)}) async-start(bf16[16,32,2048]{2,1,0:T(8,128)(2,1)} %constant_dynamic-slice_fusion), calls=%async_computation.1 | async-start | bytes 4194304 | tf_op jit(solution)/shard_map/all_to_all | solution.py:144
  109.2 91.8 %collective-permute-start = (bf16[512,2048]{1,0:T(8,128)(2,1)}, bf16[512,2048]{1,0:T(8,128)(2,1)}, u32[]{:S(2)}, u32[]{:S(2)}) collective-permute-start(bf16[512,2048]{1,0:T(8,128)(2,1)} %bitcast.2), channel_id=1, source_target_pairs={{0,1},{1,0},{2,3},{3,2},{4,5},{5,4},{6,7},{7,6},{8,9},{9,8},{10,11... | collective-permute-start | bytes 6291464 | tf_op jit(solution)/shard_map/ppermute | solution.py:18
  201.0 4.7 %copy-start.2 = (bf16[1,2048,512]{2,1,0:T(8,128)(2,1)S(1)}, bf16[1,2048,512]{2,1,0:T(8,128)(2,1)}, u32[]{:S(2)}) copy-start(bf16[1,2048,512]{2,1,0:T(8,128)(2,1)} %param.21) | copy-start | bytes 6291460
  201.0 10.1 %collective-permute-start.1 = (bf16[512,2048]{1,0:T(8,128)(2,1)}, bf16[512,2048]{1,0:T(8,128)(2,1)S(1)}, u32[]{:S(2)}, u32[]{:S(2)}) collective-permute-start(bf16[512,2048]{1,0:T(8,128)(2,1)} %bitcast.4), channel_id=1, source_target_pairs={{0,1},{1,0},{2,3},{3,2},{4,5},{5,4},{6,7},{7,6},{8,9},{9,8},{10,11... | collective-permute-start | bytes 6291464 | tf_op jit(solution)/shard_map/ppermute | solution.py:18
  205.7 5.4 %copy-start.25 = (f32[1024,512]{1,0:T(8,128)}, f32[1024,512]{1,0:T(8,128)S(1)}, u32[]{:S(2)}) copy-start(f32[1024,512]{1,0:T(8,128)S(1)} %fusion.9) | copy-start | bytes 6291460
  205.7 5.4 %copy-start.22 = (bf16[1,512,2048]{2,1,0:T(8,128)(2,1)S(1)}, bf16[1,512,2048]{2,1,0:T(8,128)(2,1)}, u32[]{:S(2)}) copy-start(bf16[1,512,2048]{2,1,0:T(8,128)(2,1)} %param.22) | copy-start | bytes 6291460
  211.1 6.2 %copy-start.27 = (f32[1024,512]{1,0:T(8,128)}, f32[1024,512]{1,0:T(8,128)S(1)}, u32[]{:S(2)}) copy-start(f32[1024,512]{1,0:T(8,128)S(1)} %fusion.13) | copy-start | bytes 6291460
  211.1 6.1 %copy-start.23 = (bf16[512,2048]{1,0:T(8,128)(2,1)}, bf16[512,2048]{1,0:T(8,128)(2,1)S(1)}, u32[]{:S(2)}) copy-start(bf16[512,2048]{1,0:T(8,128)(2,1)S(1)} %collective-permute-done.1) | copy-start | bytes 6291460
  217.3 3.0 copy-start.8
  217.3 6.8 %copy-start.10 = (bf16[1024,512]{1,0:T(8,128)(2,1)}, bf16[1024,512]{1,0:T(8,128)(2,1)S(1)}, u32[]{:S(2)}) copy-start(bf16[1024,512]{1,0:T(8,128)(2,1)S(1)} %get-tuple-element.20) | copy-start | bytes 3145732
  219.9 4.2 %collective-permute-start.2 = (bf16[512,2048]{1,0:T(8,128)(2,1)S(1)}, bf16[512,2048]{1,0:T(8,128)(2,1)S(1)}, u32[]{:S(2)}, u32[]{:S(2)}) collective-permute-start(bf16[512,2048]{1,0:T(8,128)(2,1)S(1)} %add_convert_fusion.1), channel_id=1, source_target_pairs={{0,1},{1,0},{2,3},{3,2},{4,5},{5,4},{6,7},{7,6},{8,9},{9,8},{10,11... | collective-permute-start | bytes 6291464 | tf_op jit(solution)/shard_map/ppermute | solution.py:18
  226.8 5.3 %copy-start.12 = (bf16[256,1024]{1,0:T(8,128)(2,1)S(1)}, bf16[256,1024]{1,0:T(8,128)(2,1)}, u32[]{:S(2)}) copy-start(bf16[256,1024]{1,0:T(8,128)(2,1)} %param.24) | copy-start | bytes 1572868
  226.8 8.7 %copy-start.3 = (f32[256,1024]{1,0:T(8,128)S(1)}, f32[256,1024]{1,0:T(8,128)}, u32[]{:S(2)}) copy-start(f32[256,1024]{1,0:T(8,128)} %param.26) | copy-start | bytes 3145732
  226.8 12.3 %copy-start.19 = (f32[1024]{0:T(1024)S(1)}, f32[1024]{0:T(1024)}, u32[]{:S(2)}) copy-start(f32[1024]{0:T(1024)} %param.30) | copy-start | bytes 12292
  226.8 12.3 %copy-start.17 = (bf16[4,1024]{1,0:T(4,128)(2,1)S(1)}, bf16[4,1024]{1,0:T(4,128)(2,1)}, u32[]{:S(2)}) copy-start(bf16[4,1024]{1,0:T(4,128)(2,1)} %param.27) | copy-start | bytes 24580
  226.8 62.2 %all-to-all-start.2 = ((bf16[16,32,2048]{2,1,0:T(8,128)(2,1)}), bf16[16,32,2048]{2,1,0:T(8,128)(2,1)}, u32[]{:S(2)}, u32[]{:S(2)}) async-start(bf16[16,32,2048]{2,1,0:T(8,128)(2,1)} %bitcast.12), calls=%async_computation.2 | async-start | bytes 4194304 | tf_op jit(solution)/shard_map/all_to_all | solution.py:176
  232.1 46.8 %collective-permute-start.4 = (f32[3,1024]{1,0:T(4,128)S(1)}, f32[3,1024]{1,0:T(4,128)S(1)}, u32[]{:S(2)}, u32[]{:S(2)}) collective-permute-start(f32[3,1024]{1,0:T(4,128)S(1)} %slice_convert_fusion), channel_id=1, source_target_pairs={{0,2},{2,4},{4,6},{6,8},{8,10},{10,12},{12,14},{14,16},{16,18},{18... | collective-permute-start | bytes 36872 | tf_op jit(solution)/shard_map/ppermute | solution.py:14
  235.5 98.1 %collective-permute-start.5 = (f32[1,1024]{1,0:T(1,128)S(1)}, f32[1,1024]{1,0:T(1,128)S(1)}, u32[]{:S(2)}, u32[]{:S(2)}) collective-permute-start(f32[1,1024]{1,0:T(1,128)S(1)} %slice.211), channel_id=1, source_target_pairs={{0,2},{2,4},{4,6},{6,8},{8,10},{10,12},{12,14},{14,16},{16,18},{18... | collective-permute-start | bytes 12296 | tf_op jit(solution)/shard_map/ppermute | solution.py:14
  280.4 1.6 copy-start.14
  289.0 2.6 copy-start.9
  291.5 6.2 %copy-start.24 = (bf16[512,2048]{1,0:T(8,128)(2,1)S(1)}, bf16[512,2048]{1,0:T(8,128)(2,1)}, u32[]{:S(2)}) copy-start(bf16[512,2048]{1,0:T(8,128)(2,1)} %copy-done.23) | copy-start | bytes 6291460
  291.5 6.2 %copy-start.26 = (f32[1024,512]{1,0:T(8,128)S(1)}, f32[1024,512]{1,0:T(8,128)}, u32[]{:S(2)}) copy-start(f32[1024,512]{1,0:T(8,128)} %copy-done.25) | copy-start | bytes 6291460
  291.5 6.2 %copy-start.28 = (f32[1024,512]{1,0:T(8,128)S(1)}, f32[1024,512]{1,0:T(8,128)}, u32[]{:S(2)}) copy-start(f32[1024,512]{1,0:T(8,128)} %copy-done.27) | copy-start | bytes 6291460
  291.5 11.9 %collective-permute-start.3 = (bf16[256,2048]{1,0:T(8,128)(2,1)S(1)}, bf16[256,2048]{1,0:T(8,128)(2,1)S(1)}, u32[]{:S(2)}, u32[]{:S(2)}) collective-permute-start(bf16[256,2048]{1,0:T(8,128)(2,1)S(1)} %fusion.4), channel_id=1, source_target_pairs={{0,1},{1,0},{2,3},{3,2},{4,5},{5,4},{6,7},{7,6},{8,9},{9,8},{10,11... | collective-permute-start | bytes 3145736 | tf_op jit(solution)/shard_map/ppermute | solution.py:18
  297.7 5.8 %copy-start.5 = (bf16[256,2048]{1,0:T(8,128)(2,1)S(1)}, bf16[256,2048]{1,0:T(8,128)(2,1)}, u32[]{:S(2)}) copy-start(bf16[256,2048]{1,0:T(8,128)(2,1)} %param.17) | copy-start | bytes 3145732
  297.7 6.3 %copy-start.21 = (bf16[2048,1024]{1,0:T(8,128)(2,1)S(1)}, bf16[2048,1024]{1,0:T(8,128)(2,1)}, u32[]{:S(2)}) copy-start(bf16[2048,1024]{1,0:T(8,128)(2,1)} %param.23) | copy-start | bytes 12582916
  303.4 1.0 copy-start.13
  304.5 3.1 copy-start.6
  307.5 13.8 %copy-start.7 = (bf16[256,2048]{1,0:T(8,128)(2,1)S(1)}, bf16[256,2048]{1,0:T(8,128)(2,1)}, u32[]{:S(2)}) copy-start(bf16[256,2048]{1,0:T(8,128)(2,1)} %copy-done.6) | copy-start | bytes 3145732
  314.4 12.3 %all-to-all-start.4 = ((f32[16,2,1024]{2,1,0:T(2,128)}), f32[16,2,1024]{2,1,0:T(2,128)S(1)}, u32[]{:S(2)}, u32[]{:S(2)}) async-start(f32[16,2,1024]{2,1,0:T(2,128)} %broadcast_in_dim.47), calls=%async_computation.4 | async-start | bytes 262144 | tf_op jit(solution)/shard_map/all_to_all | solution.py:24
  326.7 32.0 %all-to-all-start.3 = ((bf16[16,256,128]{2,1,0:T(8,128)(2,1)}), bf16[16,256,128]{2,1,0:T(8,128)(2,1)S(1)}, u32[]{:S(2)}, u32[]{:S(2)}) async-start(bf16[16,256,128]{2,1,0:T(8,128)(2,1)} %bitcast_bitcast_fusion), calls=%async_computation.3 | async-start | bytes 2097152 | tf_op jit(solution)/shard_map/all_to_all | solution.py:186
  333.6 5.4 %copy-start.15 = (bf16[8,128,128]{2,1,0:T(8,128)(2,1)S(1)}, bf16[8,128,128]{2,1,0:T(8,128)(2,1)}, u32[]{:S(2)}) copy-start(bf16[8,128,128]{2,1,0:T(8,128)(2,1)} %param.29) | copy-start | bytes 786436
  339.0 1.7 copy-start.16
  343.3 4.9 %copy-start.11 = (bf16[1024,512]{1,0:T(8,128)(2,1)S(1)}, bf16[1024,512]{1,0:T(8,128)(2,1)}, u32[]{:S(2)}) copy-start(bf16[1024,512]{1,0:T(8,128)(2,1)} %copy-done.10) | copy-start | bytes 3145732
  345.7 11.7 %collective-permute-start.6 = (f32[3,1024]{1,0:T(4,128)S(1)}, f32[3,1024]{1,0:T(4,128)S(1)}, u32[]{:S(2)}, u32[]{:S(2)}) collective-permute-start(f32[3,1024]{1,0:T(4,128)S(1)} %slice.261), channel_id=1, source_target_pairs={{2,0},{4,2},{6,4},{8,6},{10,8},{12,10},{14,12},{16,14},{18,16},{20... | collective-permute-start | bytes 36872 | tf_op jit(solution)/shard_map/ppermute | solution.py:14
  358.7 5.6 %copy-start.1 = (bf16[1,2048,512]{2,1,0:T(8,128)(2,1)S(1)}, bf16[1,2048,512]{2,1,0:T(8,128)(2,1)}, u32[]{:S(2)}) copy-start(bf16[1,2048,512]{2,1,0:T(8,128)(2,1)} %param.20) | copy-start | bytes 6291460
Sparse Core Ops, SparseCore 0:
  11.3 187.1 all-gather.1
where the time goes:
time: 378 us; the launch traced here: 372 us
  waiting for transfers between devices  204 us (54%)
  matrix products  64.5 us (17%)
  starting transfers between devices  42.3 us (11%)
  local copies, waits for them, and re-layouts  21.7 us (6%)
  other arithmetic  19 us (5%)
  between operations  15.1 us (4%)
  Pallas kernels  5.31 us (1%)
    all_to_all x1, waiting for transfers between devices, on_device(): lax.all_to_all(mine_grads, 'sp', split_axis=0, concat_axis=0, tiled=True)  91.7 us
    all_to_all x1, waiting for transfers between devices, on_device(): lax.all_to_all(mine_rows, 'sp', split_axis=0, concat_axis=0, tiled=True)  62.5 us
    ppermute x3, waiting for transfers between devices, passed_along(): lax.ppermute(value, axis, [(source, source + steps) for source in range(i...  42.9 us
    dot_general x5, matrix products, contract_rows(): lax.dot_general(left, right, (((0,), (0,)), ((), ())), preferred_element_...  25.8 us
    dot_general x5, matrix products, contract_cols(): lax.dot_general(left, right, (((1,), (1,)), ((), ())), preferred_element_...  12.7 us
    mul x3, local copies, waits for them, and re-layouts, on_device(): route_weight[:, :, None] * cotangent.astype(jnp.float32)[:, None, :]  10.4 us
    ppermute x3, starting transfers between devices, passed_along(): lax.ppermute(value, axis, [(source, source + steps) for source in range(i...  9.42 us
  transfers between devices with their start and end apart: 13, of which 6 were waited for; matrix products, arithmetic and copies ran while one was open for 26% of the time, Pallas kernels for 1%

commit v1 on v0

--- a/solution.py
+++ b/solution.py
@@ -1,3 +1,5 @@
+import functools
+
 import jax
 import jax.numpy as jnp
 from jax import lax
@@ -6,6 +8,310 @@
 from jax.sharding import PartitionSpec as P
 
 decay_scale = 8.0
+BF = jnp.bfloat16
+F32 = jnp.float32
+PLANES = 4
+MESH = pl.DeviceIdType.MESH
+
+
+def dot_nn(left, right):
+    return jnp.dot(left, right, preferred_element_type=F32)
+
+
+def dot_nt(left, right):
+    return lax.dot_general(left, right, (((1,), (1,)), ((), ())), preferred_element_type=F32)
+
+
+def dot_tn(left, right):
+    return lax.dot_general(left, right, (((0,), (0,)), ((), ())), preferred_element_type=F32)
+
+
+def aligned(index, size):
+    return pl.ds(pl.multiple_of(index * size, size), size)
+
+
+def local_wait(view, sem):
+    pltpu.make_async_copy(view, view, sem).wait()
+
+
+def remote(src, dst, send, recv, **where):
+    return pltpu.make_async_remote_copy(
+        src_ref=src, dst_ref=dst, send_sem=send, recv_sem=recv, device_id=where, device_id_type=MESH
+    )
+
+
+def expert_kernel(
+    count, cap,
+    tok_ref, cot_ref, place_ref, place_t_ref, weight_ref, mixer_ref, gate_w, up_w, down_w,
+    grad_ref, plane_ref, gate_g, up_g, down_g,
+    wgu, wd, send_r, send_g, rows, grads, pre, hid, xgu, own, psend, precv, tsend, back, halves,
+    dgu, ddown,
+    load_sem, bulk_sem, rows_sem, grads_sem, back_sem, mixer_sem, pair_send, pair_recv,
+):
+    me, core = lax.axis_index("sp"), lax.axis_index("tp")
+    other = 1 - core
+    peers = count // PLANES
+    zed, pos = me // peers, lax.rem(me, peers)
+    group = peers * cap
+    tokens, width = tok_ref.shape
+    half = width // 2
+    hidden = wd.shape[0]
+    mine = aligned(core, half)
+    theirs = aligned(other, half)
+
+    loads = [
+        pltpu.make_async_copy(gate_w, wgu.at[:, pl.ds(0, hidden)], load_sem.at[0]),
+        pltpu.make_async_copy(up_w, wgu.at[:, pl.ds(hidden, hidden)], load_sem.at[1]),
+        pltpu.make_async_copy(down_w, wd, load_sem.at[2]),
+    ]
+    for load in loads:
+        load.start()
+
+    barrier = pltpu.get_barrier_semaphore()
+
+    def greet(step, carry):
+        pl.semaphore_signal(
+            barrier, inc=1, device_id={"sp": lax.rem(me + step, count)}, device_id_type=MESH
+        )
+        return carry
+
+    lax.fori_loop(1, count, greet, 0)
+    pl.semaphore_signal(barrier, inc=1, device_id={"tp": other}, device_id_type=MESH)
+
+    def place(step, source, scaled):
+        plane = lax.rem(zed + (PLANES - 1 - step), PLANES)
+        span = aligned(plane, group)
+        placed = dot_nn(place_ref[span, :], source[:, mine])
+        if scaled:
+            placed = placed * weight_ref[span, :]
+        return plane, span, placed.astype(BF)
+
+    def spread(step, plane, source, target, which, sems):
+        def one(shift, carry):
+            dest = plane * peers + lax.rem(pos + shift, peers)
+            remote(
+                source.at[aligned(dest, cap)], target.at[aligned(me, cap)],
+                bulk_sem.at[which], sems.at[zed], sp=dest,
+            ).start()
+            return carry
+
+        lax.fori_loop(jnp.where(step == PLANES - 1, 1, 0), peers, one, 0)
+
+        @pl.when(step == PLANES - 1)
+        def _():
+            pltpu.make_async_copy(
+                source.at[aligned(me, cap)], target.at[aligned(me, cap)], sems.at[zed]
+            ).start()
+
+    for which, (source, sent, target, sems) in enumerate(
+        ((tok_ref, send_r, rows, rows_sem), (cot_ref, send_g, grads, grads_sem))
+    ):
+        def issue(step, carry, which=which, source=source, sent=sent, target=target, sems=sems):
+            plane, span, placed = place(step, source, which == 1)
+            sent[span, :] = placed
+            if which == 0:
+                @pl.when(step == 0)
+                def _():
+                    pl.semaphore_wait(barrier, count)
+            spread(step, plane, sent, target.at[core], which, sems)
+            return carry
+
+        lax.fori_loop(0, PLANES, issue, 0)
+
+    def share(shift, carry):
+        dest = zed * peers + lax.rem(pos + shift, peers)
+        remote(
+            mixer_ref, plane_ref.at[aligned(pos, tokens)], bulk_sem.at[3], mixer_sem.at[0], sp=dest
+        ).start()
+        return carry
+
+    lax.fori_loop(1, peers, share, 0)
+    keep = pltpu.make_async_copy(mixer_ref, plane_ref.at[aligned(pos, tokens)], mixer_sem.at[1])
+    keep.start()
+
+    def from_plane(step):
+        return lax.rem(zed + step + 1, PLANES)
+
+    def to_pair(view, slot):
+        return remote(view, view, pair_send.at[slot], pair_recv.at[slot], tp=other)
+
+    def pass_rows(step, carry):
+        span = aligned(from_plane(step), group)
+        view = rows.at[core, span]
+        local_wait(view, rows_sem.at[from_plane(step)])
+        to_pair(view, step).start()
+        return carry
+
+    lax.fori_loop(0, PLANES, pass_rows, 0)
+    for load in loads:
+        load.wait()
+
+    def forward(step, carry):
+        span = aligned(from_plane(step), group)
+        to_pair(rows.at[other, span], step).wait_recv()
+        pre[span, :] = dot_nn(rows[0, span, :], wgu[:half, :]) + dot_nn(
+            rows[1, span, :], wgu[half:, :]
+        )
+        return carry
+
+    lax.fori_loop(0, PLANES, forward, 0)
+
+    def finish(step):
+        plane = from_plane(step)
+        span = aligned(plane, group)
+        to_pair(precv.at[span], 2 * PLANES + step).wait_recv()
+        tsend[span, :] = (own[lax.rem(step, 2)] + precv[span, :].astype(F32)).astype(BF)
+
+        def one(shift, carry):
+            dest = plane * peers + lax.rem(pos + shift, peers)
+            remote(
+                tsend.at[aligned(dest, cap)], back.at[aligned(me, cap)],
+                bulk_sem.at[2], back_sem.at[zed], sp=dest,
+            ).start()
+            return carry
+
+        lax.fori_loop(jnp.where(step == PLANES - 1, 1, 0), peers, one, 0)
+
+        @pl.when(step == PLANES - 1)
+        def _():
+            pltpu.make_async_copy(
+                tsend.at[aligned(me, cap)], back.at[aligned(me, cap)], back_sem.at[zed]
+            ).start()
+
+    def backward(step, carry):
+        plane = from_plane(step)
+        span = aligned(plane, group)
+        view = grads.at[core, span]
+        local_wait(view, grads_sem.at[plane])
+        to_pair(view, PLANES + step).start()
+
+        @pl.when(step > 0)
+        def _():
+            finish(step - 1)
+
+        to_pair(grads.at[other, span], PLANES + step).wait_recv()
+        hidden_grad = dot_nt(grads[0, span, :], wd[:, :half]) + dot_nt(
+            grads[1, span, :], wd[:, half:]
+        )
+        gate = pre[span, :hidden]
+        up = pre[span, hidden:]
+        sig = jax.nn.sigmoid(gate)
+        silu = gate * sig
+        hid[span, :] = (silu * up).astype(BF)
+        xgu[span, :hidden] = (hidden_grad * up * sig * (1.0 + gate * (1.0 - sig))).astype(BF)
+        xgu[span, hidden:] = (hidden_grad * silu).astype(BF)
+        psend[span, :] = dot_nt(xgu[span, :], wgu[theirs, :]).astype(BF)
+        remote(
+            psend.at[span], precv.at[span], pair_send.at[2 * PLANES + step],
+            pair_recv.at[2 * PLANES + step], tp=other,
+        ).start()
+        own[lax.rem(step, 2)] = dot_nt(xgu[span, :], wgu[mine, :])
+        return carry
+
+    lax.fori_loop(0, PLANES, backward, 0)
+    finish(PLANES - 1)
+
+    tile = 256
+    tiles = half // tile
+
+    for side in range(2):
+        def weight_tile(step, carry, side=side):
+            columns = aligned(step, tile)
+            spot = pl.ds(pl.multiple_of(side * half + step * tile, tile), tile)
+            dgu[spot, :] = dot_tn(rows[side, :, columns], xgu[...]).astype(BF)
+            ddown[:, spot] = dot_tn(hid[...], grads[side, :, columns]).astype(BF)
+            return carry
+
+        lax.fori_loop(0, tiles, weight_tile, 0)
+
+    stores = [
+        pltpu.make_async_copy(dgu.at[:, pl.ds(0, hidden)], gate_g, load_sem.at[0]),
+        pltpu.make_async_copy(dgu.at[:, pl.ds(hidden, hidden)], up_g, load_sem.at[1]),
+        pltpu.make_async_copy(ddown, down_g, load_sem.at[2]),
+    ]
+    for store in stores:
+        store.start()
+
+    def gather(step, carry):
+        plane = from_plane(step)
+        local_wait(back.at[aligned(plane, group)], back_sem.at[plane])
+        return carry
+
+    lax.fori_loop(0, PLANES, gather, 0)
+    moe = dot_nn(place_t_ref[...], back[...])
+    halves[core] = (moe + cot_ref[:, mine].astype(F32)).astype(BF)
+    last = to_pair(halves.at[core], 3 * PLANES)
+    last.start()
+    grad_ref[:, mine] = halves[core]
+    to_pair(halves.at[other], 3 * PLANES).wait_recv()
+    grad_ref[:, theirs] = halves[other]
+
+    sent_rows = (count - 1) * cap
+    for which in range(3):
+        local_wait(send_r.at[pl.ds(0, sent_rows)], bulk_sem.at[which])
+    shared = plane_ref.at[pl.ds(0, (peers - 1) * tokens)]
+    local_wait(shared, bulk_sem.at[3])
+    local_wait(shared, mixer_sem.at[0])
+    keep.wait()
+    for slot in range(2 * PLANES):
+        to_pair(rows.at[0, pl.ds(0, group)], slot).wait_send()
+    for slot in range(2 * PLANES, 3 * PLANES):
+        to_pair(psend.at[pl.ds(0, group)], slot).wait_send()
+    last.wait_send()
+    for store in stores:
+        store.wait()
+
+
+def expert_exchange(tok, cot, place, place_t, weight, mixer, gate_w, up_w, down_w):
+    count = lax.axis_size("sp")
+    tokens, width = tok.shape
+    slots = place.shape[0]
+    cap = slots // count
+    half = width // 2
+    hidden = gate_w.shape[1]
+    peers = count // PLANES
+    group = peers * cap
+    vmem, anywhere = pl.BlockSpec(memory_space=pltpu.VMEM), pl.BlockSpec(memory_space=pl.ANY)
+    dma = pltpu.SemaphoreType.DMA
+    flops = 2 * slots * width * hidden * 8
+    return pl.pallas_call(
+        functools.partial(expert_kernel, count, cap),
+        in_specs=[vmem] * 6 + [anywhere] * 3,
+        out_specs=[vmem] + [anywhere] * 4,
+        out_shape=[
+            jax.ShapeDtypeStruct((tokens, width), BF),
+            jax.ShapeDtypeStruct((peers * tokens, mixer.shape[1]), BF),
+            jax.ShapeDtypeStruct(gate_w.shape, BF),
+            jax.ShapeDtypeStruct(up_w.shape, BF),
+            jax.ShapeDtypeStruct(down_w.shape, BF),
+        ],
+        scratch_shapes=[
+            pltpu.VMEM((width, 2 * hidden), BF),
+            pltpu.VMEM((hidden, width), BF),
+            pltpu.VMEM((slots, half), BF),
+            pltpu.VMEM((slots, half), BF),
+            pltpu.VMEM((2, slots, half), BF),
+            pltpu.VMEM((2, slots, half), BF),
+            pltpu.VMEM((slots, 2 * hidden), F32),
+            pltpu.VMEM((slots, hidden), BF),
+            pltpu.VMEM((slots, 2 * hidden), BF),
+            pltpu.VMEM((2, group, half), F32),
+            pltpu.VMEM((slots, half), BF),
+            pltpu.VMEM((slots, half), BF),
+            pltpu.VMEM((slots, half), BF),
+            pltpu.VMEM((slots, half), BF),
+            pltpu.VMEM((2, tokens, half), BF),
+            pltpu.VMEM((width, 2 * hidden), BF),
+            pltpu.VMEM((hidden, width), BF),
+            dma((3,)), dma((4,)), dma((PLANES,)), dma((PLANES,)), dma((PLANES,)), dma((2,)),
+            dma((3 * PLANES + 1,)), dma((3 * PLANES + 1,)),
+        ],
+        compiler_params=pltpu.CompilerParams(
+            collective_id=0, has_side_effects=True, vmem_limit_bytes=62 * 1024 * 1024
+        ),
+        cost_estimate=pl.CostEstimate(flops=flops, bytes_accessed=20 << 20, transcendentals=0),
+        name="expert_exchange",
+    )(tok, cot, place, place_t, weight, mixer, gate_w, up_w, down_w)
 
 
 def passed_along(value, axis, steps):
@@ -115,73 +421,19 @@
     gate_float = gate_input.astype(jnp.float32)
     gelu_value, gelu_back = jax.vjp(jax.nn.gelu, gate_float)
     mixer_out = (states * gelu_value).astype(jnp.bfloat16)
-    mixer_all = lax.all_gather(mixer_out, "sp", axis=0, tiled=True)
     flat_ids = expert_ids.reshape(-1)
     onehot = (flat_ids[:, None] == jnp.arange(experts, dtype=jnp.int32)[None, :]).astype(jnp.int32)
     slot_rank = jnp.sum((jnp.cumsum(onehot, axis=0) - onehot) * onehot, axis=1)
-    target = flat_ids * capacity + slot_rank
+    pair_slots = (flat_ids * capacity + slot_rank).reshape(tok_rows, top_count)
     slot_iota = jnp.arange(slot_count, dtype=jnp.int32)
-    placing = (slot_iota[:, None] == target[None, :]).astype(jnp.bfloat16)
-    pair_slots = target.reshape(tok_rows, top_count)
-    placing_tok = jnp.any(slot_iota[:, None, None] == pair_slots[None, :, :], axis=2).astype(
-        jnp.bfloat16
-    )
-    scaled = (route_weight[:, :, None] * cotangent.astype(jnp.float32)[:, None, :]).astype(
-        jnp.bfloat16
-    )
-    scaled = scaled.reshape(tok_rows * top_count, width)
-    send_rows = jnp.dot(placing_tok, moe_input, preferred_element_type=jnp.float32).astype(
-        jnp.bfloat16
-    )
-    send_rows = send_rows.reshape(experts, capacity, width)
-    send_grads = jnp.dot(placing, scaled, preferred_element_type=jnp.float32).astype(jnp.bfloat16)
-    send_grads = send_grads.reshape(experts, capacity, width)
-    share_size = capacity // cores
-    offset = lax.axis_index("tp") * share_size
-    mine_rows = lax.dynamic_slice_in_dim(send_rows, offset, share_size, 1)
-    mine_grads = lax.dynamic_slice_in_dim(send_grads, offset, share_size, 1)
-    got_rows = lax.all_to_all(mine_rows, "sp", split_axis=0, concat_axis=0, tiled=True)
-    got_grads = lax.all_to_all(mine_grads, "sp", split_axis=0, concat_axis=0, tiled=True)
-    got_rows = got_rows.reshape(experts * share_size, width)
-    got_grads = got_grads.reshape(experts * share_size, width)
-    rows_in = jnp.concatenate([got_rows, swapped(got_rows, "tp")], axis=0)
-    grads_in = jnp.concatenate([got_grads, swapped(got_grads, "tp")], axis=0)
-    weight_gate = gate_proj[0]
-    weight_up = up_proj[0]
-    weight_down = down_proj[0]
-    gate_pre = jnp.dot(rows_in, weight_gate, preferred_element_type=jnp.float32)
-    up_pre = jnp.dot(rows_in, weight_up, preferred_element_type=jnp.float32)
-    sigmoid_gate = jax.nn.sigmoid(gate_pre)
-    silu_gate = gate_pre * sigmoid_gate
-    hidden = (silu_gate * up_pre).astype(jnp.bfloat16)
-    down_grad = contract_rows(hidden, grads_in)
-    hidden_grad = contract_cols(grads_in, weight_down)
-    gate_pre_grad = (
-        hidden_grad * up_pre * sigmoid_gate * (1.0 + gate_pre * (1.0 - sigmoid_gate))
-    ).astype(jnp.bfloat16)
-    up_pre_grad = (hidden_grad * silu_gate).astype(jnp.bfloat16)
-    gate_weight_grad = contract_rows(rows_in, gate_pre_grad)
-    up_weight_grad = contract_rows(rows_in, up_pre_grad)
-    half = experts * share_size
-    other_part = (
-        contract_cols(gate_pre_grad[half:], weight_gate)
-        + contract_cols(up_pre_grad[half:], weight_up)
-    ).astype(jnp.bfloat16)
-    arrived_part = swapped(other_part, "tp").astype(jnp.float32)
-    own_part = contract_cols(gate_pre_grad[:half], weight_gate) + contract_cols(
-        up_pre_grad[:half], weight_up
-    )
-    shared = (own_part + arrived_part).astype(jnp.bfloat16)
-    shared, mixer_all = lax.optimization_barrier((shared, mixer_all))
-    back_half = lax.all_to_all(
-        shared.reshape(experts, share_size, width), "sp", split_axis=0, concat_axis=0, tiled=True
-    )
-    placing_half = lax.dynamic_slice_in_dim(
-        placing_tok.reshape(experts, capacity, tok_rows), offset, share_size, 1
-    ).reshape(half, tok_rows)
-    moe_part = contract_rows(placing_half, back_half.reshape(half, width)).astype(jnp.bfloat16)
-    moe_grad = moe_part.astype(jnp.float32) + swapped(moe_part, "tp").astype(jnp.float32)
-    input_grad = (moe_grad + cotangent.astype(jnp.float32)).astype(jnp.bfloat16)
+    placing = slot_iota[:, None, None] == pair_slots[None, :, :]
+    place = jnp.any(placing, axis=2).astype(jnp.bfloat16)
+    place_t = jnp.any(pair_slots[:, :, None] == slot_iota[None, None, :], axis=1).astype(jnp.bfloat16)
+    weight = jnp.sum(jnp.where(placing, route_weight[None], 0.0), axis=(1, 2))[:, None]
+    input_grad, mixer_plane, gate_weight_grad, up_weight_grad, down_grad = expert_exchange(
+        moe_input, cotangent, place, place_t, weight, mixer_out, gate_proj[0], up_proj[0], down_proj[0]
+    )
+    mixer_all = lax.all_gather(mixer_out, "sp", axis=0, tiled=True)
     column_share = width // experts
     grad_columns = lax.all_to_all(
         input_grad.reshape(tok_rows, experts, column_share).transpose(1, 0, 2),

time: 378 us -> 333 us (0.88); the launches traced: 372 us -> 332 us
  Pallas kernels: 5.31 us -> 225 us
  waiting for transfers between devices: 204 us -> 14 us
  matrix products: 64.5 us -> 13.5 us
  starting transfers between devices: 42.3 us -> 27.1 us
  local copies, waits for them, and re-layouts: 21.7 us -> 17.9 us
    pallas_call x0 -> x1, Pallas kernels: none -> 220 us  [expert_exchange(): pl.pallas_call(functools.partial(expert_kernel, count, cap), in_specs=[vm...]
    all_to_all x3 -> x0, waiting for transfers between devices: 154 us -> none  [the longest x1 91.7 us: on_device(): lax.all_to_all(mine_grads, 'sp', split_axis=0, concat_axis=0, tiled=True)]
    ppermute x3, waiting for transfers between devices: 42.9 us -> 9.51 us  [passed_along(): lax.ppermute(value, axis, [(source, source + steps) for source in range(i...]
    dot_general x9 -> x0, matrix products: 29.8 us -> none  [the longest x5 12.7 us: contract_cols(): lax.dot_general(left, right, (((1,), (1,)), ((), ())), preferred_element_...]
    dot_general x5 -> x1, matrix products: 25.8 us -> 5.61 us  [contract_rows(): lax.dot_general(left, right, (((0,), (0,)), ((), ())), preferred_element_...]
    all_to_all x3 -> x0, starting transfers between devices: 18.6 us -> none  [the longest x1 7.28 us: on_device(): lax.all_to_all(mine_rows, 'sp', split_axis=0, concat_axis=0, tiled=True)]
    mul x3 -> x0, local copies, waits for them, and re-layouts: 10.4 us -> none  [on_device(): route_weight[:, :, None] * cotangent.astype(jnp.float32)[:, None, :]]
    unnamed x60 -> x43, local copies, waits for them, and re-layouts: 0.89 us -> 9 us
  transfers between devices with their start and end apart: 13 -> 6, of which waited for: 6 -> 2; matrix products, arithmetic and copies ran while one was open for 26% -> 10% of each run, Pallas kernels for 1% -> 68%
where the time goes in v1:
time: 333 us; the launch traced here: 332 us
  Pallas kernels  225 us (68%)
  starting transfers between devices  27.1 us (8%)
  other arithmetic  19.8 us (6%)
  local copies, waits for them, and re-layouts  17.9 us (5%)
  between operations  14.4 us (4%)
  waiting for transfers between devices  14 us (4%)
  matrix products  13.5 us (4%)
    pallas_call x1, Pallas kernels, expert_exchange(): pl.pallas_call(functools.partial(expert_kernel, count, cap), in_specs=[vm...  220 us
    all_to_all x1, starting transfers between devices, carried_in(): lax.all_to_all(jnp.broadcast_to(pair[None], (count,) + pair.shape), axis,...  11.6 us
    ppermute x3, waiting for transfers between devices, passed_along(): lax.ppermute(value, axis, [(source, source + steps) for source in range(i...  9.51 us
    ppermute x3, starting transfers between devices, passed_along(): lax.ppermute(value, axis, [(source, source + steps) for source in range(i...  9.24 us
    unnamed x43, local copies, waits for them, and re-layouts  9 us
    unnamed x2, other arithmetic  6.78 us
  transfers between devices with their start and end apart: 6, of which 2 were waited for; matrix products, arithmetic and copies ran while one was open for 10% of the time, Pallas kernels for 68%

profile of v1, /device:TPU:14, one launch (start us, length us, event | category | flops | bytes accessed | tf_op | source)
XLA Modules:
  0.0 332.3 jit_solution(16317063074581550528)
XLA Ops:
  7.2 0.0 copy-start
  7.2 0.0 copy-start.1
  7.2 0.0 all-gather.2.cloned.1.call-start
  7.3 2.7 multiply_convert_fusion.1.mixer_ref
  10.0 0.0 all-gather.2.cloned.1.call-update
  10.0 3.4 %collective-permute-start = (f32[3,1024]{1,0:T(4,128)S(1)}, f32[3,1024]{1,0:T(4,128)S(1)}, u32[]{:S(2)}, u32[]{:S(2)}) collective-permute-start(f32[3,1024]{1,0:T(4,128)S(1)} %slice_convert_fusion), channel_id=1, source_target_pairs={{0,2},{2,4},{4,6},{6,8},{8,10},{10,12},{12,14},{14,16},{16,18},{18... | collective-permute-start | bytes 36872 | tf_op jit(solution)/shard_map/ppermute | solution.py:320
  13.4 0.6 slice.195
  14.0 3.4 %collective-permute-start.1 = (f32[1,1024]{1,0:T(1,128)}, f32[1,1024]{1,0:T(1,128)}, u32[]{:S(2)}, u32[]{:S(2)}) collective-permute-start(f32[1,1024]{1,0:T(1,128)} %slice.195), channel_id=1, source_target_pairs={{0,2},{2,4},{4,6},{6,8},{8,10},{10,12},{12,14},{14,16},{16,18},{18... | collective-permute-start | bytes 12296 | tf_op jit(solution)/shard_map/ppermute | solution.py:320
  17.5 0.1 copy.73
  17.6 0.1 eq.62
  17.7 0.1 eq.66
  17.9 1.2 reduce-window.6
  19.1 0.2 slice_reduce_fusion
  19.3 0.1 fusion.59
  19.4 0.1 reduce_sum.21
  19.6 0.1 copy.76
  19.7 0.4 fusion
  20.0 0.9 convert_element_type.45.place_ref
  20.9 0.3 fusion.1
  21.2 0.9 convert_element_type.46.place_t_ref
  22.1 0.3 select_reduce_fusion
  22.4 1.0 copy.77.weight_ref
  23.4 220.3 %expert_exchange.1 = (bf16[256,2048]{1,0:T(8,128)(2,1)}, bf16[1024,1024]{1,0:T(8,128)(2,1)}, bf16[2048,512]{1,0:T(8,128)(2,1)}, bf16[2048,512]{1,0:T(8,128)(2,1)}, bf16[512,2048]{1,0:T(8,128)(2,1)}) custom-call(bf16[256,2048]{1,0:T(8,128)(2,1)} %tok_ref.1, bf16[256,2048]{1,0:T(8,128)(2,1)} %cot_ref.1, bf16[1024,256]{1,0:T(8,128)(2,1)} %convert_element_type.45.place_ref, ...), custom_call_target="tpu_custom_call" | custom-call | flops 17179869184 | bytes 20971520 | tf_op jit(solution)/shard_map/expert_exchange/pallas_call | solution.py:277
  243.7 0.0 copy-start.9
  243.7 2.6 bitcast_bitcast_fusion
  246.3 5.2 %fusion.11 = (bf16[256,1024]{1,0:T(8,128)(2,1)}, f32[256,1024]{1,0:T(8,128)}) fusion(bf16[256,1024]{1,0:T(8,128)(2,1)S(1)} %copy-done.9, f32[256,1024]{1,0:T(8,128)S(1)} %copy-done.1, bf16[256,2048]{1,0:T(8,128)(2,1)S(1)} %copy-done.3, bf16[2048,1024]{1,0:T(8,128)(2,1)} %param.23), kind=kOutput, calls=%fused_computation.26 | convolution fusion | flops 1080033280 | bytes 8388608 | tf_op jit(solution)/shard_map/dot_general | solution.py:446
  251.5 0.6 add_compare_fusion
  252.1 0.1 convert_element_type.51
  252.3 0.0 collective-permute-done
  252.3 1.5 convert_bitcast_fusion
  253.8 0.5 fusion.8
  254.3 0.3 copy-done.10
  254.6 0.3 copy.91
  254.9 0.9 copy-done.2
  255.8 1.2 fusion.56.decay_ref
  256.9 5.2 %reverse_scan.1 = (f32[256,1024]{1,0:T(8,128)}, f32[256,1024]{1,0:T(8,128)}) custom-call(f32[256,1024]{1,0:T(8,128)} %fusion.56.decay_ref, f32[256,1024]{1,0:T(8,128)} %get-tuple-element.25.grad_ref), custom_call_target="tpu_custom_call" | custom-call | flops 786432 | bytes 4194304 | tf_op jit(solution)/shard_map/reverse_scan/pallas_call | solution.py:372
  262.2 0.8 slice_multiply_fusion.2
  263.0 0.7 broadcast_in_dim.63
  263.7 11.6 %all-to-all-start.1 = ((f32[16,2,1024]{2,1,0:T(2,128)}), f32[16,2,1024]{2,1,0:T(2,128)S(1)}, u32[]{:S(2)}, u32[]{:S(2)}) async-start(f32[16,2,1024]{2,1,0:T(2,128)} %broadcast_in_dim.63), calls=%async_computation.1 | async-start | bytes 262144 | tf_op jit(solution)/shard_map/all_to_all | solution.py:330
  275.3 0.5 fusion.5
  275.8 0.3 copy.92
  276.1 4.5 %all-to-all-done.1 = f32[16,2,1024]{2,1,0:T(2,128)S(1)} async-done(((f32[16,2,1024]{2,1,0:T(2,128)}), f32[16,2,1024]{2,1,0:T(2,128)S(1)}, u32[]{:S(2)}, u32[]{:S(2)}) %all-to-all-start.1) | async-done | bytes 131104 | tf_op jit(solution)/shard_map/all_to_all | solution.py:330
  280.6 6.3 %all-to-all-start = ((bf16[16,256,128]{2,1,0:T(8,128)(2,1)}), bf16[16,256,128]{2,1,0:T(8,128)(2,1)S(1)}, u32[]{:S(2)}, u32[]{:S(2)}) async-start(bf16[16,256,128]{2,1,0:T(8,128)(2,1)} %bitcast_bitcast_fusion), calls=%async_computation | async-start | bytes 2097152 | tf_op jit(solution)/shard_map/all_to_all | solution.py:438
  286.9 0.1 fusion.63
  287.0 0.1 add_select_fusion
  287.0 0.0 collective-permute-done.1
  287.1 5.3 %fusion.44 = (bf16[32,8,8,128]{3,2,1,0:T(8,128)(2,1)S(1)}, f32[256,1024]{1,0:T(8,128)}, bf16[32,8,8,128]{3,2,1,0:T(8,128)(2,1)}) fusion(f32[256,1024]{1,0:T(8,128)S(1)} %copy.92, f32[256,1024]{1,0:T(8,128)} %get-tuple-element.22, f32[256,1024]{1,0:T(8,128)} %param.31, f32[256,1024]{1,0:T(8,128)S(1)} %copy.91, f32[1024]{0:T(1024)S(1)} %broadcast_multiply_fusion, ...), kind=kLoop, calls=%fused_computation.69 | loop fusion | flops 7340032 | bytes 9445632
  292.4 0.3 fusion.45
  292.7 1.3 copy.94
  294.0 1.4 fusion.48
  295.4 1.3 copy.93
  296.7 2.3 add_add_fusion
  299.0 2.5 collective-permute-start.2
  301.5 9.5 %collective-permute-done.2 = f32[3,1024]{1,0:T(4,128)S(1)} collective-permute-done((f32[3,1024]{1,0:T(4,128)S(1)}, f32[3,1024]{1,0:T(4,128)S(1)}, u32[]{:S(2)}, u32[]{:S(2)}) %collective-permute-start.2) | collective-permute-done | bytes 12320 | tf_op jit(solution)/shard_map/ppermute | solution.py:320
  311.0 1.3 fusion.17
  312.2 0.0 all-to-all-done
  312.2 5.6 %fusion.66 = f32[128,1024]{1,0:T(8,128)} fusion(bf16[4096,128]{1,0:T(8,128)(2,1)S(1)} %bitcast.105, bf16[4096,1024]{1,0:T(8,128)(2,1)} %all-gather.2.cloned.1.call-done), kind=kOutput, calls=%fused_computation.106 | convolution fusion | flops 1073741824 | bytes 9961472 | tf_op jit(solution)/shard_map/dot_general | solution.py:386
  317.9 1.3 copy.122
  319.2 1.0 copy-done.6
  320.2 1.3 copy.123
  321.5 1.0 copy-done.5
  322.6 1.3 copy.124
  323.9 0.6 copy-done.4
  324.5 1.0 copy.125
  (41 shorter events, 0.2 us)
Async XLA Ops:
  7.2 268.1 %copy-start = (bf16[8,128,128]{2,1,0:T(8,128)(2,1)S(1)}, bf16[8,128,128]{2,1,0:T(8,128)(2,1)}, u32[]{:S(2)}) copy-start(bf16[8,128,128]{2,1,0:T(8,128)(2,1)} %param.29) | copy-start | bytes 786436
  7.2 6.3 %copy-start.1 = (f32[256,1024]{1,0:T(8,128)S(1)}, f32[256,1024]{1,0:T(8,128)}, u32[]{:S(2)}) copy-start(f32[256,1024]{1,0:T(8,128)} %param.26) | copy-start | bytes 3145732
  7.2 2.8 copy-start.8
  7.2 10.2 %copy-start.16 = (s32[256,2]{0,1:T(2,128)S(1)}, s32[256,2]{0,1:T(2,128)}, u32[]{:S(2)}) copy-start(s32[256,2]{0,1:T(2,128)} %param.18) | copy-start | bytes 6148
  7.2 305.0 %all-gather.2.cloned.1.call-start = ((), (), s32[]{:S(2)}) async-start(), calls=%async_computation.2 | async-start | bytes 8912896 | tf_op jit(solution)/shard_map/all_gather | solution.py:436
  10.0 12.1 %copy-start.18 = (f32[256,2]{0,1:T(2,128)S(1)}, f32[256,2]{0,1:T(2,128)}, u32[]{:S(2)}) copy-start(f32[256,2]{0,1:T(2,128)} %param.19) | copy-start | bytes 6148
  10.0 13.4 %copy-start.17 = (f32[1024]{0:T(1024)S(1)}, f32[1024]{0:T(1024)}, u32[]{:S(2)}) copy-start(f32[1024]{0:T(1024)} %param.30) | copy-start | bytes 12292
  10.0 13.4 %copy-start.15 = (bf16[4,1024]{1,0:T(4,128)(2,1)S(1)}, bf16[4,1024]{1,0:T(4,128)(2,1)}, u32[]{:S(2)}) copy-start(bf16[4,1024]{1,0:T(4,128)(2,1)} %param.27) | copy-start | bytes 24580
  10.0 242.2 %collective-permute-start = (f32[3,1024]{1,0:T(4,128)S(1)}, f32[3,1024]{1,0:T(4,128)S(1)}, u32[]{:S(2)}, u32[]{:S(2)}) collective-permute-start(f32[3,1024]{1,0:T(4,128)S(1)} %slice_convert_fusion), channel_id=1, source_target_pairs={{0,2},{2,4},{4,6},{6,8},{8,10},{10,12},{12,14},{14,16},{16,18},{18... | collective-permute-start | bytes 36872 | tf_op jit(solution)/shard_map/ppermute | solution.py:320
  14.0 273.0 %collective-permute-start.1 = (f32[1,1024]{1,0:T(1,128)}, f32[1,1024]{1,0:T(1,128)}, u32[]{:S(2)}, u32[]{:S(2)}) collective-permute-start(f32[1,1024]{1,0:T(1,128)} %slice.195), channel_id=1, source_target_pairs={{0,2},{2,4},{4,6},{6,8},{8,10},{10,12},{12,14},{14,16},{16,18},{18... | collective-permute-start | bytes 12296 | tf_op jit(solution)/shard_map/ppermute | solution.py:320
  23.4 228.9 %copy-start.13 = (f32[1,1024]{1,0:T(1,128)}, f32[1,1024]{1,0:T(1,128)S(1)}, u32[]{:S(2)}) copy-start(f32[1,1024]{1,0:T(1,128)S(1)} %get-tuple-element.60) | copy-start | bytes 12292
  243.7 2.6 copy-start.3
  243.7 2.6 copy-start.9
  252.1 1.6 copy-start.12
  253.8 0.8 copy-start.10
  254.5 1.2 copy-start.2
  255.8 19.5 %copy-start.11 = (bf16[32,8,8,128]{3,2,1,0:T(8,128)(2,1)S(1)}, bf16[32,8,8,128]{3,2,1,0:T(8,128)(2,1)}, u32[]{:S(2)}) copy-start(bf16[32,8,8,128]{3,2,1,0:T(8,128)(2,1)} %copy-done.10) | copy-start | bytes 1572868
  263.7 16.9 %all-to-all-start.1 = ((f32[16,2,1024]{2,1,0:T(2,128)}), f32[16,2,1024]{2,1,0:T(2,128)S(1)}, u32[]{:S(2)}, u32[]{:S(2)}) async-start(f32[16,2,1024]{2,1,0:T(2,128)} %broadcast_in_dim.63), calls=%async_computation.1 | async-start | bytes 262144 | tf_op jit(solution)/shard_map/all_to_all | solution.py:330
  280.6 31.7 %all-to-all-start = ((bf16[16,256,128]{2,1,0:T(8,128)(2,1)}), bf16[16,256,128]{2,1,0:T(8,128)(2,1)S(1)}, u32[]{:S(2)}, u32[]{:S(2)}) async-start(bf16[16,256,128]{2,1,0:T(8,128)(2,1)} %bitcast_bitcast_fusion), calls=%async_computation | async-start | bytes 2097152 | tf_op jit(solution)/shard_map/all_to_all | solution.py:438
  296.7 14.3 %copy-start.14 = (f32[1,1024]{1,0:T(1,128)S(1)}, f32[1,1024]{1,0:T(1,128)}, u32[]{:S(2)}) copy-start(f32[1,1024]{1,0:T(1,128)} %copy-done.13) | copy-start | bytes 12292
  299.0 12.0 %collective-permute-start.2 = (f32[3,1024]{1,0:T(4,128)S(1)}, f32[3,1024]{1,0:T(4,128)S(1)}, u32[]{:S(2)}, u32[]{:S(2)}) collective-permute-start(f32[3,1024]{1,0:T(4,128)S(1)} %slice.241), channel_id=1, source_target_pairs={{2,0},{4,2},{6,4},{8,6},{10,8},{12,10},{14,12},{16,14},{18,16},{20... | collective-permute-start | bytes 36872 | tf_op jit(solution)/shard_map/ppermute | solution.py:320
  312.2 5.6 %copy-start.7 = (bf16[2048,512]{1,0:T(8,128)(2,1)S(1)}, bf16[2048,512]{1,0:T(8,128)(2,1)}, u32[]{:S(2)}) copy-start(bf16[2048,512]{1,0:T(8,128)(2,1)} %get-tuple-element.13) | copy-start | bytes 6291460
  317.9 2.3 copy-start.6
  320.2 2.3 copy-start.5
  322.5 2.0 copy-start.4
Sparse Core Ops, SparseCore 0:
  10.8 210.7 all-gather.1

commit v2 on v1

--- a/solution.py
+++ b/solution.py
@@ -314,84 +314,244 @@
     )(tok, cot, place, place_t, weight, mixer, gate_w, up_w, down_w)
 
 
+SEGMENTS = 8
+
+
+def tail_kernel(
+    count,
+    grad_ref, cols_ref, plane_w, out_w, gelu_ref, slope_ref, decay_ref, first_ref, second_ref,
+    third_ref, decay_w, input_w, taps_ref,
+    gate_out, recur_out, weight_out,
+    outw, mixer, cols, part, send_part, got_part, state, decays, local, cumul, conv_grad, pair, pieces,
+    load_sem, bulk_sem, cols_sem, part_sem, carry_send, carry_recv, halo_sem,
+):
+    me = lax.axis_index("sp")
+    peers = count // PLANES
+    zed, pos = me // peers, lax.rem(me, peers)
+    tokens, channels = gelu_ref.shape
+    share = weight_out.shape[0]
+    span = tokens // SEGMENTS
+
+    loads = [
+        pltpu.make_async_copy(out_w, outw, load_sem.at[0]),
+        pltpu.make_async_copy(plane_w, mixer, load_sem.at[1]),
+        pltpu.make_async_copy(cols_ref.at[pos], cols.at[aligned(pos, tokens)], load_sem.at[2]),
+    ]
+    for load in loads:
+        load.start()
+
+    barrier = pltpu.get_barrier_semaphore()
+
+    def greet(step, carry):
+        pl.semaphore_signal(
+            barrier, inc=1, device_id={"sp": lax.rem(me + step, count)}, device_id_type=MESH
+        )
+        return carry
+
+    lax.fori_loop(1, count, greet, 0)
+    pl.semaphore_wait(barrier, count - 1)
+
+    def send_cols(shift, carry):
+        place = lax.rem(pos + shift, peers)
+        remote(
+            cols_ref.at[place], cols.at[aligned(pos, tokens)], bulk_sem.at[0], cols_sem.at[0],
+            sp=zed * peers + place,
+        ).start()
+        return carry
+
+    lax.fori_loop(1, peers, send_cols, 0)
+
+    loads[0].wait()
+    mixer_grad = dot_nn(grad_ref[...], outw[...])
+    gate_out[...] = (mixer_grad * slope_ref[...]).astype(BF)
+    width = decay_w.shape[1]
+    blocks = range(channels // width)
+
+    def lanes(block):
+        return slice(block * width, (block + 1) * width)
+
+    for block in blocks:
+        state[block] = mixer_grad[:, lanes(block)] * gelu_ref[:, lanes(block)]
+        decays[block] = decay_ref[:, lanes(block)]
+
+    def scan(step, carry):
+        rows = pl.ds(span - 1 - step, SEGMENTS, stride=span)
+        after = []
+        for block in blocks:
+            product, total, decay = carry[block]
+            product = product * decay
+            total = state[block, rows, :] + decay * total
+            cumul[block, rows, :] = product
+            local[block, rows, :] = total
+            after.append((product, total, decays[block, rows, :]))
+        return after
+
+    start = []
+    for block in blocks:
+        rows = pl.ds(span - 1, SEGMENTS, stride=span)
+        decay = decays[block, rows, :]
+        total = state[block, rows, :]
+        product = decay * 0.0 + 1.0
+        cumul[block, rows, :] = product
+        local[block, rows, :] = total
+        start.append((product, total, decay))
+    ended = lax.fori_loop(1, span, scan, start)
+    product = jnp.concatenate([ended[block][0] * ended[block][2] for block in blocks], axis=1)
+    total = jnp.concatenate([ended[block][1] * ended[block][2] for block in blocks], axis=1)
+    whole, entry = product[SEGMENTS - 1 :], total[SEGMENTS - 1 :]
+    for segment in range(SEGMENTS - 2, -1, -1):
+        row = slice(segment, segment + 1)
+        whole = whole * product[row]
+        entry = total[row] + product[row] * entry
+    pair[0:1, :] = whole
+    pair[1:2, :] = entry
+
+    def carry_copy(dest):
+        return remote(pair, pieces.at[me], carry_send.at[dest], carry_recv.at[me], sp=dest)
+
+    def send_carry(step, carry):
+        carry_copy(me - 1 - step).start()
+        return carry
+
+    lax.fori_loop(0, me, send_carry, 0)
+
+    def take_carry(step, entering):
+        source = count - 1 - step
+        local_wait(pieces.at[source], carry_recv.at[source])
+        return pieces[source, 0:1, :] * entering + pieces[source, 1:2, :]
+
+    entering = lax.fori_loop(
+        0, count - 1 - me, take_carry, jnp.zeros((1, channels), F32)
+    )
+    enter = []
+    for segment in range(SEGMENTS - 1, -1, -1):
+        enter.append(entering)
+        row = slice(segment, segment + 1)
+        entering = total[row] + product[row] * entering
+    enter = jnp.concatenate(enter[::-1], axis=0)
+
+    for block in blocks:
+        at = lanes(block)
+        spread = jnp.broadcast_to(enter[:, None, at], (SEGMENTS, span, width)).reshape(tokens, width)
+        carried = local[block] + cumul[block] * spread
+        both = jnp.concatenate(
+            [(carried * first_ref[:, at]).astype(BF), (carried * second_ref[:, at]).astype(BF)],
+            axis=1,
+        )
+        maps = jnp.concatenate([decay_w[block], input_w[block]], axis=1)
+        conv_grad[0:tokens, at] = carried * third_ref[:, at] + dot_nt(both, maps)
+
+    halo = pl.ds(tokens, 8)
+
+    def halo_copy():
+        return remote(
+            conv_grad.at[pl.ds(0, 8)], conv_grad.at[halo], halo_sem.at[0], halo_sem.at[1], sp=me - 1
+        )
+
+    @pl.when(me > 0)
+    def _():
+        halo_copy().start()
+
+    @pl.when(me == count - 1)
+    def _():
+        conv_grad[halo, :] = jnp.zeros((8, channels), F32)
+
+    loads[1].wait()
+    loads[2].wait()
+    local_wait(cols.at[pl.ds(0, (peers - 1) * tokens)], cols_sem.at[0])
+    part[...] = dot_tn(cols[...], mixer[...])
+    send_part[...] = part[...].astype(BF)
+
+    def send_block(shift, carry):
+        plane = lax.rem(zed + shift, PLANES)
+        remote(
+            send_part.at[aligned(plane, share)], got_part.at[aligned(zed, share)],
+            bulk_sem.at[1], part_sem.at[zed], sp=plane * peers + pos,
+        ).start()
+        return carry
+
+    lax.fori_loop(1, PLANES, send_block, 0)
+
+    def taps_over(low, high):
+        total = taps_ref[0:1, :] * conv_grad[low + 3 : high + 3, :]
+        for tap in range(1, 4):
+            total = total + taps_ref[tap : tap + 1, :] * conv_grad[low + 3 - tap : high + 3 - tap, :]
+        recur_out[low:high, :] = total.astype(BF)
+
+    taps_over(0, tokens - 16)
+
+    @pl.when(me < count - 1)
+    def _():
+        local_wait(conv_grad.at[halo], halo_sem.at[1])
+
+    taps_over(tokens - 16, tokens)
+
+    summed = part[aligned(zed, share), :]
+    for shift in range(1, PLANES):
+        plane = lax.rem(zed + shift, PLANES)
+        local_wait(got_part.at[aligned(plane, share)], part_sem.at[plane])
+        summed = summed + got_part[aligned(plane, share), :].astype(F32)
+    weight_out[...] = summed
+
+    local_wait(cols.at[pl.ds(0, (peers - 1) * tokens)], bulk_sem.at[0])
+    local_wait(got_part.at[pl.ds(0, (PLANES - 1) * share)], bulk_sem.at[1])
+
+    def sent_carry(step, carry):
+        carry_copy(me - 1 - step).wait_send()
+        return carry
+
+    lax.fori_loop(0, me, sent_carry, 0)
+
+    @pl.when(me > 0)
+    def _():
+        halo_copy().wait_send()
+
+
+def tail_exchange(
+    grad, cols, plane, out_weight, gelu, slope, decay, first, second, third, decay_w, input_w, taps
+):
+    count = lax.axis_size("sp")
+    tokens, channels = gelu.shape
+    peers = count // PLANES
+    total_share = cols.shape[2]
+    share = total_share // PLANES
+    vmem, anywhere = pl.BlockSpec(memory_space=pltpu.VMEM), pl.BlockSpec(memory_space=pl.ANY)
+    dma = pltpu.SemaphoreType.DMA
+    flops = 4 * tokens * out_weight.shape[0] * channels
+    return pl.pallas_call(
+        functools.partial(tail_kernel, count),
+        in_specs=[vmem] * 2 + [anywhere] * 2 + [vmem] * 9,
+        out_specs=[vmem] * 3,
+        out_shape=[
+            jax.ShapeDtypeStruct((tokens, channels), BF),
+            jax.ShapeDtypeStruct((tokens, channels), BF),
+            jax.ShapeDtypeStruct((share, channels), F32),
+        ],
+        scratch_shapes=[
+            pltpu.VMEM(out_weight.shape, BF),
+            pltpu.VMEM(plane.shape, BF),
+            pltpu.VMEM((peers * tokens, total_share), BF),
+            pltpu.VMEM((total_share, channels), F32),
+            pltpu.VMEM((total_share, channels), BF),
+            pltpu.VMEM((total_share, channels), BF),
+            *[pltpu.VMEM((decay_w.shape[0], tokens, decay_w.shape[1]), F32)] * 4,
+            pltpu.VMEM((tokens + 8, channels), F32),
+            pltpu.VMEM((2, channels), F32),
+            pltpu.VMEM((count, 2, channels), F32),
+            dma((3,)), dma((2,)), dma((1,)), dma((PLANES,)), dma((count,)), dma((count,)), dma((2,)),
+        ],
+        compiler_params=pltpu.CompilerParams(
+            collective_id=1, has_side_effects=True, vmem_limit_bytes=48 * 1024 * 1024
+        ),
+        cost_estimate=pl.CostEstimate(flops=flops, bytes_accessed=16 << 20, transcendentals=0),
+        name="tail_exchange",
+    )(grad, cols, plane, out_weight, gelu, slope, decay, first, second, third, decay_w, input_w, taps)
+
+
 def passed_along(value, axis, steps):
     count = lax.axis_size(axis)
     initial, last = (max(0, -steps), min(count, count - steps))
     return lax.ppermute(value, axis, [(source, source + steps) for source in range(initial, last)])
-
-
-def swapped(value, axis):
-    return lax.ppermute(value, axis, [(0, 1), (1, 0)])
-
-
-def carried_in(product, total, axis):
-    count, mine = (lax.axis_size(axis), lax.axis_index(axis))
-    pair = jnp.stack([product, total])
-    pieces = lax.all_to_all(
-        jnp.broadcast_to(pair[None], (count,) + pair.shape),
-        axis,
-        split_axis=0,
-        concat_axis=0,
-        tiled=True,
-    )
-    entering = jnp.zeros_like(total)
-    for position in range(count - 1, 0, -1):
-        longer = pieces[position, 0] * entering + pieces[position, 1]
-        entering = jnp.where(position > mine, longer, entering)
-    return entering
-
-
-def scan_kernel(decay_ref, grad_ref, product_ref, local_ref):
-    rows, lanes = decay_ref.shape
-    group = 8
-    last = rows // group - 1
-
-    def step(index, carry):
-        product, total, decay = carry
-        start = pl.multiple_of((last - index) * group, group)
-        decays = decay_ref[pl.ds(start, group), :]
-        grads = grad_ref[pl.ds(start, group), :]
-        products, totals = ([None] * group, [None] * group)
-        for row in range(group - 1, -1, -1):
-            product = product * decay
-            total = grads[row : row + 1] + decay * total
-            decay = decays[row : row + 1]
-            products[row], totals[row] = (product, total)
-        product_ref[pl.ds(start, group), :] = jnp.concatenate(products, axis=0)
-        local_ref[pl.ds(start, group), :] = jnp.concatenate(totals, axis=0)
-        return (product, total, decay)
-
-    one = jnp.ones((1, lanes), jnp.float32)
-    lax.fori_loop(0, last + 1, step, (one, jnp.zeros_like(one), one))
-
-
-def reverse_scan(decay, grad):
-    rows, channels = decay.shape
-    width = 512 if channels % 512 == 0 else channels
-    block = pl.BlockSpec((rows, width), lambda index: (0, index))
-    return pl.pallas_call(
-        scan_kernel,
-        grid=(channels // width,),
-        in_specs=[block, block],
-        out_specs=[block, block],
-        out_shape=[jax.ShapeDtypeStruct(decay.shape, jnp.float32)] * 2,
-        cost_estimate=pl.CostEstimate(
-            flops=3 * rows * channels, bytes_accessed=16 * rows * channels, transcendentals=0
-        ),
-        name="reverse_scan",
-    )(decay, grad)
-
-
-def contract_rows(left, right):
-    return lax.dot_general(
-        left, right, (((0,), (0,)), ((), ())), preferred_element_type=jnp.float32
-    )
-
-
-def contract_cols(left, right):
-    return lax.dot_general(
-        left, right, (((1,), (1,)), ((), ())), preferred_element_type=jnp.float32
-    )
 
 
 def on_device(
@@ -413,104 +573,69 @@
     decay_extra,
 ):
     experts = lax.axis_size("sp")
-    cores = lax.axis_size("tp")
     tok_rows, width = moe_input.shape
     top_count = expert_ids.shape[1]
     capacity = max(2, 4 * tok_rows // experts)
     slot_count = experts * capacity
-    gate_float = gate_input.astype(jnp.float32)
-    gelu_value, gelu_back = jax.vjp(jax.nn.gelu, gate_float)
-    mixer_out = (states * gelu_value).astype(jnp.bfloat16)
+    gelu_value, gelu_back = jax.vjp(jax.nn.gelu, gate_input.astype(F32))
+    mixer_out = (states * gelu_value).astype(BF)
+    slope = states * gelu_back(jnp.ones_like(gelu_value))[0]
+    channels = recur_input.shape[1]
+    recur_float = recur_input.astype(F32)
+    before = passed_along(jnp.concatenate([recur_float[-3:], states[-1:]], axis=0), "sp", 1)
+    extended = jnp.concatenate([before[:3], recur_float], axis=0)
+    taps = conv_taps.astype(F32)
+    conv = taps[0] * extended[0:tok_rows]
+    for tap_index in range(1, 4):
+        conv = conv + taps[tap_index] * extended[tap_index : tap_index + tok_rows]
+    blocks = decay_gate_w.shape[0]
+    block_width = decay_gate_w.shape[1]
+    conv_blocks = conv.astype(BF).reshape(tok_rows, blocks, block_width)
+    decay_pre = jnp.einsum(
+        "tbi,bij->tbj", conv_blocks, decay_gate_w, preferred_element_type=F32
+    ).reshape(tok_rows, channels)
+    input_pre = jnp.einsum(
+        "tbi,bij->tbj", conv_blocks, input_gate_w, preferred_element_type=F32
+    ).reshape(tok_rows, channels)
+    recur_gate = jax.nn.sigmoid(decay_pre)
+    input_gate = jax.nn.sigmoid(input_pre)
+    positions = lax.axis_index("sp") * tok_rows + jnp.arange(tok_rows, dtype=jnp.int32)
+    first_row = (positions == 0)[:, None]
+    rate = -decay_scale * decay_rate[None, :]
+    log_decay = rate * recur_gate + decay_extra
+    decay_value = jnp.exp(log_decay)
+    mult = jnp.where(first_row, 1.0, jnp.sqrt(-jnp.expm1(2.0 * log_decay)))
+    prev_states = jnp.concatenate([before[3:], states[:-1]], axis=0)
+    log_factor = prev_states * decay_value - jnp.where(
+        first_row, 0.0, input_gate * conv * decay_value * decay_value / mult
+    )
+    decay_factor = log_factor * rate * recur_gate * (1.0 - recur_gate)
+    input_factor = mult * conv * input_gate * (1.0 - input_gate)
+    conv_factor = mult * input_gate
+
     flat_ids = expert_ids.reshape(-1)
     onehot = (flat_ids[:, None] == jnp.arange(experts, dtype=jnp.int32)[None, :]).astype(jnp.int32)
     slot_rank = jnp.sum((jnp.cumsum(onehot, axis=0) - onehot) * onehot, axis=1)
     pair_slots = (flat_ids * capacity + slot_rank).reshape(tok_rows, top_count)
     slot_iota = jnp.arange(slot_count, dtype=jnp.int32)
     placing = slot_iota[:, None, None] == pair_slots[None, :, :]
-    place = jnp.any(placing, axis=2).astype(jnp.bfloat16)
-    place_t = jnp.any(pair_slots[:, :, None] == slot_iota[None, None, :], axis=1).astype(jnp.bfloat16)
+    place = jnp.any(placing, axis=2).astype(BF)
+    place_t = jnp.any(pair_slots[:, :, None] == slot_iota[None, None, :], axis=1).astype(BF)
     weight = jnp.sum(jnp.where(placing, route_weight[None], 0.0), axis=(1, 2))[:, None]
     input_grad, mixer_plane, gate_weight_grad, up_weight_grad, down_grad = expert_exchange(
         moe_input, cotangent, place, place_t, weight, mixer_out, gate_proj[0], up_proj[0], down_proj[0]
     )
-    mixer_all = lax.all_gather(mixer_out, "sp", axis=0, tiled=True)
-    column_share = width // experts
-    grad_columns = lax.all_to_all(
-        input_grad.reshape(tok_rows, experts, column_share).transpose(1, 0, 2),
-        "sp",
-        split_axis=0,
-        concat_axis=0,
-        tiled=True,
-    ).reshape(experts * tok_rows, column_share)
-    out_weight_grad = contract_rows(grad_columns, mixer_all)
-    mixer_grad = jnp.dot(input_grad, out_weight, preferred_element_type=jnp.float32)
-    gate_grad = gelu_back(mixer_grad * states)[0].astype(jnp.bfloat16)
-    state_grad = mixer_grad * gelu_value
-    channels = recur_input.shape[1]
-    prev_inputs, prev_state = passed_along(
-        (recur_input[-3:].astype(jnp.float32), states[-1:]), "sp", 1
+    peers = experts // PLANES
+    cols = input_grad.reshape(tok_rows, PLANES, peers, width // experts)
+    cols = cols.transpose(2, 0, 1, 3).reshape(peers, tok_rows, width // peers)
+    gate_grad, recur_grad, out_weight_grad = tail_exchange(
+        input_grad, cols, mixer_plane, out_weight, gelu_value, slope, decay_value,
+        decay_factor, input_factor, conv_factor, decay_gate_w, input_gate_w, taps,
     )
-    extended = jnp.concatenate([prev_inputs, recur_input.astype(jnp.float32)], axis=0)
-    taps = conv_taps.astype(jnp.float32)
-    conv = taps[0] * extended[0:tok_rows]
-    for tap_index in range(1, 4):
-        conv = conv + taps[tap_index] * extended[tap_index : tap_index + tok_rows]
-    blocks = decay_gate_w.shape[0]
-    block_width = decay_gate_w.shape[1]
-    conv_blocks = conv.astype(jnp.bfloat16).reshape(tok_rows, blocks, block_width)
-    decay_pre = jnp.einsum(
-        "tbi,bij->tbj", conv_blocks, decay_gate_w, preferred_element_type=jnp.float32
-    ).reshape(tok_rows, channels)
-    input_pre = jnp.einsum(
-        "tbi,bij->tbj", conv_blocks, input_gate_w, preferred_element_type=jnp.float32
-    ).reshape(tok_rows, channels)
-    recur_gate = jax.nn.sigmoid(decay_pre)
-    input_gate = jax.nn.sigmoid(input_pre)
-    positions = lax.axis_index("sp") * tok_rows + jnp.arange(tok_rows, dtype=jnp.int32)
-    first_row = (positions == 0)[:, None]
-    log_decay = -decay_scale * recur_gate * decay_rate[None, :] + decay_extra
-    decay_value = jnp.exp(log_decay)
-    mult = jnp.where(first_row, 1.0, jnp.sqrt(-jnp.expm1(2.0 * log_decay)))
-    prev_states = jnp.concatenate([prev_state, states[:-1]], axis=0)
-    cumul, local_values = reverse_scan(decay_value, state_grad)
-    entering = carried_in(decay_value[0] * cumul[0], decay_value[0] * local_values[0], "sp")
-    carried_grad = local_values + cumul * entering[None, :]
-    log_grad = carried_grad * prev_states * decay_value - jnp.where(
-        first_row, 0.0, carried_grad * input_gate * conv * decay_value * decay_value / mult
-    )
-    decay_pre_grad = (
-        log_grad * (-decay_scale * decay_rate[None, :]) * recur_gate * (1.0 - recur_gate)
-    ).astype(jnp.bfloat16)
-    input_pre_grad = (carried_grad * mult * conv * input_gate * (1.0 - input_gate)).astype(
-        jnp.bfloat16
-    )
-    conv_grad = (
-        carried_grad * mult * input_gate
-        + jnp.einsum(
-            "tbj,bij->tbi",
-            decay_pre_grad.reshape(tok_rows, blocks, block_width),
-            decay_gate_w,
-            preferred_element_type=jnp.float32,
-        ).reshape(tok_rows, channels)
-        + jnp.einsum(
-            "tbj,bij->tbi",
-            input_pre_grad.reshape(tok_rows, blocks, block_width),
-            input_gate_w,
-            preferred_element_type=jnp.float32,
-        ).reshape(tok_rows, channels)
-    )
-    next_grads = passed_along(conv_grad[:3], "sp", -1)
-    grad_extended = jnp.concatenate([conv_grad, next_grads], axis=0)
-    recur_float = taps[0] * grad_extended[3 : 3 + tok_rows]
-    for tap_index in range(1, 4):
-        recur_float = (
-            recur_float + taps[tap_index] * grad_extended[3 - tap_index : 3 - tap_index + tok_rows]
-        )
-    recur_grad = recur_float.astype(jnp.bfloat16)
     return (
-        gate_weight_grad.astype(jnp.bfloat16)[None],
-        up_weight_grad.astype(jnp.bfloat16)[None],
-        down_grad.astype(jnp.bfloat16)[None],
+        gate_weight_grad[None],
+        up_weight_grad[None],
+        down_grad[None],
         out_weight_grad,
         input_grad,
         recur_grad,

time: 333 us -> 255 us (0.77)
  starting transfers between devices: 27.1 us -> 3.4 us
  Pallas kernels: 225 us -> 204 us
  waiting for transfers between devices: 14 us -> 0.01 us
  between operations: 14.4 us -> 0.86 us
  matrix products: 13.5 us -> 4.04 us
  local copies, waits for them, and re-layouts: 17.9 us -> 23 us
    pallas_call x1, Pallas kernels: 220 us -> 145 us  [expert_exchange(): pl.pallas_call(functools.partial(expert_kernel, count, cap), in_specs=[vm...]
    pallas_call x1, Pallas kernels: 5.23 us -> 58.8 us  [tail_exchange(): pl.pallas_call(functools.partial(tail_kernel, count), in_specs=[vmem] * 2...]
    all_to_all x2 -> x0, starting transfers between devices: 17.9 us -> none  [the longest x1 11.6 us: carried_in(): lax.all_to_all(jnp.broadcast_to(pair[None], (count,) + pair.shape), axis,...]
    dot_general x4 -> x0, matrix products: 12.6 us -> none  [the longest x1 5.61 us: contract_rows(): lax.dot_general(left, right, (((0,), (0,)), ((), ())), preferred_element_...]
    ppermute x3 -> x1, waiting for transfers between devices: 9.51 us -> 0.01 us  [passed_along(): lax.ppermute(value, axis, [(source, source + steps) for source in range(i...]
    mul x2 -> x3, other arithmetic: 0.8 us -> 7.74 us  [the longest x1 5.81 us: on_device(): input_factor = mult * conv * input_gate * (1.0 - input_gate)]
    ppermute x3 -> x1, starting transfers between devices: 9.24 us -> 3.4 us  [passed_along(): lax.ppermute(value, axis, [(source, source + steps) for source in range(i...]
    div x2, local copies, waits for them, and re-layouts: 0.66 us -> 5.16 us  [on_device(): recur_gate = jax.nn.sigmoid(decay_pre)]
  transfers between devices with their start and end apart: 6 -> 1, of which waited for: 2 -> 0; matrix products, arithmetic and copies ran while one was open for 10% -> 6% of each run, Pallas kernels for 68% -> 57%
where the time goes in v2:
time: 255 us; the launch traced here: 253 us
  Pallas kernels  204 us (80%)
  local copies, waits for them, and re-layouts  23 us (9%)
  other arithmetic  17.6 us (7%)
  matrix products  4.04 us (2%)
  starting transfers between devices  3.4 us (1%)
    pallas_call x1, Pallas kernels, expert_exchange(): pl.pallas_call(functools.partial(expert_kernel, count, cap), in_specs=[vm...  145 us
    pallas_call x1, Pallas kernels, tail_exchange(): pl.pallas_call(functools.partial(tail_kernel, count), in_specs=[vmem] * 2...  58.8 us
    unnamed x34, local copies, waits for them, and re-layouts  10.7 us
    mul x1, other arithmetic, on_device(): input_factor = mult * conv * input_gate * (1.0 - input_gate)  5.81 us
    div x2, local copies, waits for them, and re-layouts, on_device(): recur_gate = jax.nn.sigmoid(decay_pre)  5.16 us
  transfers between devices with their start and end apart: 1, of which 0 were waited for; matrix products, arithmetic and copies ran while one was open for 6% of the time, Pallas kernels for 57%

profile of v2, /device:TPU:14, one launch (start us, length us, event | category | flops | bytes accessed | tf_op | source)
XLA Modules:
  0.0 252.7 jit_solution(9603451873278168471)
XLA Ops:
  0.6 0.0 copy-start.3
  0.6 0.0 copy-start.12
  0.7 0.0 copy-start.9
  0.7 0.9 slice.46
  1.5 0.7 slice.58
  2.3 3.4 %collective-permute-start = (f32[4,1024]{1,0:T(4,128)S(1)}, f32[4,1024]{1,0:T(4,128)S(1)}, u32[]{:S(2)}, u32[]{:S(2)}) collective-permute-start(f32[4,1024]{1,0:T(4,128)S(1)} %pad_maximum_fusion.1), channel_id=1, source_target_pairs={{0,2},{2,4},{4,6},{6,8},{8,10},{10,12},{12,14},{14,16},{16,18},{18... | collective-permute-start | bytes 49160 | tf_op jit(solution)/shard_map/ppermute | solution.py:554
  5.7 0.8 copy.62
  6.5 0.1 eq.62
  6.7 0.1 eq.66
  6.8 1.2 reduce-window.6
  8.0 0.2 slice_reduce_fusion
  8.2 0.1 fusion.37
  8.3 0.1 reduce_sum.21
  8.5 0.1 copy.65
  8.6 0.7 multiply_add_fusion.1
  9.2 0.4 fusion
  9.6 0.3 fusion.1
  9.9 0.9 convert_element_type.30.place_ref
  10.8 0.9 convert_element_type.31.place_t_ref
  11.7 0.0 copy-done.12
  11.7 0.3 select_reduce_fusion
  12.0 1.0 copy.66.weight_ref
  13.0 0.0 copy-done.3
  13.0 0.0 copy-done.9
  13.0 0.0 copy-start.10
  13.0 0.0 copy-start.11
  13.0 1.9 fusion.11
  14.9 0.0 copy-done.10
  14.9 0.0 copy-done.11
  15.0 0.0 copy-start.7
  15.0 145.0 %expert_exchange.1 = (bf16[256,2048]{1,0:T(8,128)(2,1)}, bf16[1024,1024]{1,0:T(8,128)(2,1)}, bf16[2048,512]{1,0:T(8,128)(2,1)}, bf16[2048,512]{1,0:T(8,128)(2,1)}, bf16[512,2048]{1,0:T(8,128)(2,1)}) custom-call(bf16[256,2048]{1,0:T(8,128)(2,1)} %tok_ref.1, bf16[256,2048]{1,0:T(8,128)(2,1)} %cot_ref.1, bf16[1024,256]{1,0:T(8,128)(2,1)} %convert_element_type.30.place_ref, ...), custom_call_target="tpu_custom_call" | custom-call | flops 17179869184 | bytes 20971520 | tf_op jit(solution)/shard_map/expert_exchange/pallas_call | solution.py:277
  160.0 0.0 copy-start
  160.0 0.0 copy-done.7
  160.0 1.1 convert_element_type.35
  161.1 0.5 copy-done
  161.6 0.7 reshape.76
  162.3 1.4 copy.90
  163.7 0.0 copy-start.1
  163.7 1.7 reshape.77.cols_ref
  165.4 0.0 collective-permute-done
  165.4 4.1 %convert_bitcast_fusion = (bf16[32,8,8,128]{3,2,1,0:T(8,128)(2,1)S(1)}, f32[256,1024]{1,0:T(8,128)}) fusion(f32[256,1024]{1,0:T(8,128)} %convert_element_type.35, f32[1024]{0:T(1024)S(1)} %bitcast.62, f32[3,1024]{1,0:T(4,128)S(1)} %bitcast.57, f32[1024]{0:T(1024)S(1)} %bitcast.61, f32[1024]{0:T(1024)S(1)} %bitcast.60, f32[1024]{0:T(1024)S(1)} %bitcast.59), kind=kLoop, calls=%fused_computation.52 | loop fusion | flops 2883584 | bytes 2650112
  169.5 0.0 copy-start.8
  169.5 0.0 copy-done.1
  169.5 1.5 fusion.5
  170.9 0.0 copy-done.8
  170.9 2.5 %copy.77 = f32[256,1024]{1,0:T(8,128)} copy(f32[256,1024]{0,1:T(8,128)} %bitcast.56) | data formatting | bytes 2097152 | tf_op jit(solution)/shard_map/div | solution.py:600
  173.5 2.6 %fusion.8 = f32[8,256,128]{1,2,0:T(8,128)} fusion(bf16[8,128,128]{2,1,0:T(8,128)(2,1)} %decay_w.1, bf16[32,8,8,128]{3,2,1,0:T(8,128)(2,1)} %copy-done.8), kind=kOutput, calls=%fused_computation.21 | convolution fusion | flops 67895296 | bytes 1835008 | tf_op jit(solution)/shard_map/tbi,bij->tbj/dot_general | solution.py:594
  176.0 2.6 %copy.76 = f32[256,1024]{1,0:T(8,128)} copy(f32[256,1024]{0,1:T(8,128)} %bitcast.55) | data formatting | bytes 2097152 | tf_op jit(solution)/shard_map/div | solution.py:600
  178.7 0.0 copy-start.2
  178.7 5.8 %subtract_multiply_fusion = (f32[256,1024]{1,0:T(8,128)}, f32[256,1024]{1,0:T(8,128)}, f32[256,1024]{1,0:T(8,128)}, f32[256,1024]{1,0:T(8,128)}) fusion(f32[256,1024]{1,0:T(8,128)} %copy.77, f32[256,1024]{1,0:T(8,128)} %get-tuple-element.24, f32[256,1024]{1,0:T(8,128)} %param.31, f32[256,1024]{1,0:T(8,128)} %copy.76, f32[1024]{0:T(1024)S(1)} %broadcast_multiply_fusion, ...), kind=kLoop, calls=%fused_computation.46 | loop fusion | flops 5767168 | bytes 9441536 | tf_op jit(solution)/shard_map/mul | solution.py:613
  184.5 0.0 copy-done.2
  184.5 0.0 copy-start.6
  184.5 58.8 %tail_exchange.1 = (bf16[256,1024]{1,0:T(8,128)(2,1)S(1)}, bf16[256,1024]{1,0:T(8,128)(2,1)S(1)}, f32[128,1024]{1,0:T(8,128)S(1)}) custom-call(bf16[256,2048]{1,0:T(8,128)(2,1)S(1)} %copy-done, bf16[4,256,512]{2,1,0:T(8,128)(2,1)S(1)} %reshape.77.cols_ref, bf16[1024,1024]{1,0:T(8,128)(2,1)} %get-tuple-element.19.plane_w, bf16[2048,1024]{1,0:T(8,128)(2,1)} %out_w.1, ...), custom_call_target="tpu_custom_call" | custom-call | flops 2147483648 | bytes 16777216 | tf_op jit(solution)/shard_map/tail_exchange/pallas_call | solution.py:521
  243.4 0.0 copy-done.6
  243.4 0.0 copy-start.5
  243.4 1.3 copy.98
  244.7 1.0 copy-done.5
  245.7 1.3 copy.99
  247.0 1.0 copy-done.4
  248.1 1.3 copy.100
  249.4 0.8 copy.101
  250.2 1.0 copy.102
  251.1 0.8 copy.103
  251.9 0.8 copy.104
  (10 shorter events, 0.1 us)
Async XLA Ops:
  0.6 12.4 %copy-start.3 = (f32[256,1024]{1,0:T(8,128)S(1)}, f32[256,1024]{1,0:T(8,128)}, u32[]{:S(2)}) copy-start(f32[256,1024]{1,0:T(8,128)} %param.26) | copy-start | bytes 3145732
  0.6 11.0 %copy-start.12 = (f32[256,2]{0,1:T(2,128)S(1)}, f32[256,2]{0,1:T(2,128)}, u32[]{:S(2)}) copy-start(f32[256,2]{0,1:T(2,128)} %param.19) | copy-start | bytes 6148
  0.7 12.3 %copy-start.9 = (bf16[256,1024]{1,0:T(8,128)(2,1)S(1)}, bf16[256,1024]{1,0:T(8,128)(2,1)}, u32[]{:S(2)}) copy-start(bf16[256,1024]{1,0:T(8,128)(2,1)} %param.25) | copy-start | bytes 1572868
  2.3 163.1 %collective-permute-start = (f32[4,1024]{1,0:T(4,128)S(1)}, f32[4,1024]{1,0:T(4,128)S(1)}, u32[]{:S(2)}, u32[]{:S(2)}) collective-permute-start(f32[4,1024]{1,0:T(4,128)S(1)} %pad_maximum_fusion.1), channel_id=1, source_target_pairs={{0,2},{2,4},{4,6},{6,8},{8,10},{10,12},{12,14},{14,16},{16,18},{18... | collective-permute-start | bytes 49160 | tf_op jit(solution)/shard_map/ppermute | solution.py:554
  13.0 1.9 copy-start.10
  13.0 2.0 copy-start.11
  15.0 145.1 %copy-start.7 = (bf16[256,1024]{1,0:T(8,128)(2,1)S(1)}, bf16[256,1024]{1,0:T(8,128)(2,1)}, u32[]{:S(2)}) copy-start(bf16[256,1024]{1,0:T(8,128)(2,1)} %param.24) | copy-start | bytes 1572868
  160.0 1.6 copy-start
  163.7 5.8 %copy-start.1 = (bf16[8,128,128]{2,1,0:T(8,128)(2,1)S(1)}, bf16[8,128,128]{2,1,0:T(8,128)(2,1)}, u32[]{:S(2)}) copy-start(bf16[8,128,128]{2,1,0:T(8,128)(2,1)} %input_w.1) | copy-start | bytes 786436
  169.5 1.5 copy-start.8
  178.7 5.8 %copy-start.2 = (bf16[8,128,128]{2,1,0:T(8,128)(2,1)S(1)}, bf16[8,128,128]{2,1,0:T(8,128)(2,1)}, u32[]{:S(2)}) copy-start(bf16[8,128,128]{2,1,0:T(8,128)(2,1)} %decay_w.1) | copy-start | bytes 786436
  184.5 58.9 %copy-start.6 = (bf16[2048,512]{1,0:T(8,128)(2,1)S(1)}, bf16[2048,512]{1,0:T(8,128)(2,1)}, u32[]{:S(2)}) copy-start(bf16[2048,512]{1,0:T(8,128)(2,1)} %get-tuple-element.15) | copy-start | bytes 6291460
  243.4 2.3 copy-start.5
  245.7 2.3 copy-start.4

commit v3 on v2

v3 whole, which is shorter than its diff:
```python
import functools

import jax
import jax.numpy as jnp
from jax import lax
from jax.experimental import pallas as pl
from jax.experimental.pallas import tpu as pltpu
from jax.sharding import PartitionSpec as P

decay_scale = 8.0
BF = jnp.bfloat16
F32 = jnp.float32
PLANES = 4
SEGMENTS = 8
LANES = 128
MESH = pl.DeviceIdType.MESH


def dot_nn(left, right):
    return jnp.dot(left, right, preferred_element_type=F32)


def dot_nt(left, right):
    return lax.dot_general(left, right, (((1,), (1,)), ((), ())), preferred_element_type=F32)


def dot_tn(left, right):
    return lax.dot_general(left, right, (((0,), (0,)), ((), ())), preferred_element_type=F32)


def aligned(index, size):
    return pl.ds(pl.multiple_of(index * size, size), size)


def local_wait(view, sem):
    pltpu.make_async_copy(view, view, sem).wait()


def remote(src, dst, send, recv, **where):
    return pltpu.make_async_remote_copy(
        src_ref=src, dst_ref=dst, send_sem=send, recv_sem=recv, device_id=where, device_id_type=MESH
    )


def iota(shape, axis):
    return lax.broadcasted_iota(jnp.int32, shape, axis)


def fallen(rise):
    series = 1.0 - rise * (1.0 / 7.0)
    for order in range(6, 1, -1):
        series = 1.0 - rise * (1.0 / order) * series
    return jnp.where(rise < 0.25, rise * series, 1.0 - jnp.exp(-rise))


def whole_kernel(
    count, cap,
    tok_ref, cot_ref, ids_ref, route_ref, decay_w, input_w, taps_ref, rate_ref,
    gate_w, up_w, down_w, out_w, recur_in, gate_in, states_in, extra_in,
    gate_g, up_g, down_g, weight_out, grad_ref, recur_out, gate_out, plane_ref,
    wgu, wd, place_t, parts, send_r, send_g, rg, pre, hid, xgu, own, psend, precv, back, halves,
    mixer, cols, send_part, got_part, gelu, slope, first, second, third, decays, cumul, local,
    conv_grad, shifted, prev_in, prev_state, pair, pieces, products,
    load_sem, bulk_sem, rows_sem, grads_sem, back_sem, mixer_sem, pair_send, pair_recv,
    before_sem, cols_sem, part_sem, carry_send, carry_recv, halo_sem,
):
    me, core = lax.axis_index("sp"), lax.axis_index("tp")
    other = 1 - core
    peers = count // PLANES
    zed, pos = me // peers, lax.rem(me, peers)
    group = peers * cap
    tokens, width = tok_ref.shape
    slots = count * cap
    half = width // 2
    hidden = wd.shape[0]
    channels = states_in.shape[1]
    blocks = channels // LANES
    segment_rows = tokens // SEGMENTS
    mine, theirs = aligned(core, half), aligned(other, half)
    rows, grads = rg.at[pl.ds(0, 2)], rg.at[pl.ds(2, 2)]

    loads = [
        pltpu.make_async_copy(gate_w, wgu.at[:, pl.ds(0, hidden)], load_sem.at[0]),
        pltpu.make_async_copy(up_w, wgu.at[:, pl.ds(hidden, hidden)], load_sem.at[1]),
        pltpu.make_async_copy(down_w, wd, load_sem.at[2]),
    ]
    inputs = [
        pltpu.make_async_copy(states_in, own.at[0], load_sem.at[3]),
        pltpu.make_async_copy(extra_in, own.at[1], load_sem.at[4]),
        pltpu.make_async_copy(recur_in, psend.at[0], load_sem.at[5]),
        pltpu.make_async_copy(gate_in, psend.at[1], load_sem.at[6]),
    ]
    for load in inputs + loads:
        load.start()

    barrier = pltpu.get_barrier_semaphore()

    def greet(step, carry):
        pl.semaphore_signal(
            barrier, inc=1, device_id={"sp": lax.rem(me + step, count)}, device_id_type=MESH
        )
        return carry

    lax.fori_loop(1, count, greet, 0)
    pl.semaphore_signal(barrier, inc=1, device_id={"tp": other}, device_id_type=MESH)

    ids, route = ids_ref[...], route_ref[...]
    expert = iota((tokens, LANES), 1)
    chosen = [ids[:, k : k + 1] == expert for k in range(2)]
    member = jnp.where(chosen[0] | chosen[1], 1.0, 0.0).astype(BF)
    earlier = (iota((tokens, tokens), 0) > iota((tokens, tokens), 1)).astype(F32).astype(BF)
    rank = dot_nn(earlier, member).astype(BF)
    low = iota((LANES, slots), 0) * cap
    column = iota((LANES, slots), 1)
    widen = jnp.where((column >= low) & (column < low + cap), 1.0, 0.0).astype(BF)
    owner = dot_nn(iota((8, LANES), 1).astype(F32).astype(BF), widen)[0:1]
    place_in = iota((1, slots), 1).astype(F32) - owner * float(cap)
    taken = (dot_nn(member, widen) > 0.5) & (dot_nn(rank, widen) == place_in)
    place_t[...] = jnp.where(taken, 1.0, 0.0).astype(BF)
    scale = jnp.where(chosen[0], route[:, 0:1], 0.0) + jnp.where(chosen[1], route[:, 1:2], 0.0)
    for piece in range(3):
        rounded = scale.astype(BF)
        parts[:, piece * LANES : (piece + 1) * LANES] = rounded
        scale = scale - rounded.astype(F32)

    pl.semaphore_wait(barrier, count)

    keep_rows = 16
    before = [
        remote(
            recur_in.at[pl.ds(tokens - keep_rows, keep_rows)], prev_in,
            before_sem.at[0], before_sem.at[1], sp=me + 1,
        ),
        remote(
            states_in.at[pl.ds(tokens - 8, 8)], prev_state,
            before_sem.at[2], before_sem.at[3], sp=me + 1,
        ),
    ]

    @pl.when(me < count - 1)
    def _():
        for copy in before:
            copy.start()

    def place(step, source, scaled):
        plane = lax.rem(zed + (PLANES - 1 - step), PLANES)
        span = aligned(plane, group)
        chosen_t = place_t[:, span]
        placed = dot_tn(chosen_t, source[:, mine])
        if scaled:
            sums = dot_tn(chosen_t, parts[...])
            sums = sums[:, :LANES] + sums[:, LANES : 2 * LANES] + sums[:, 2 * LANES :]
            slot = iota((group, LANES), 0) + plane * group
            low = iota((group, LANES), 1) * cap
            own_lane = (slot >= low) & (slot < low + cap)
            placed = placed * jnp.sum(jnp.where(own_lane, sums, 0.0), axis=1, keepdims=True)
        return plane, span, placed.astype(BF)

    def spread(step, plane, source, target, which, sem):
        def one(shift, carry):
            dest = plane * peers + lax.rem(pos + shift, peers)
            remote(
                source.at[aligned(dest, cap)], target.at[aligned(me, cap)],
                bulk_sem.at[which], sem, sp=dest,
            ).start()
            return carry

        lax.fori_loop(jnp.where(step == PLANES - 1, 1, 0), peers, one, 0)

        @pl.when(step == PLANES - 1)
        def _():
            pltpu.make_async_copy(
                source.at[aligned(me, cap)], target.at[aligned(me, cap)], sem
            ).start()

    for which, (source, sent, target, sems) in enumerate(
        ((tok_ref, send_r, rows, rows_sem), (cot_ref, send_g, grads, grads_sem))
    ):
        def issue(step, carry, which=which, source=source, sent=sent, target=target, sems=sems):
            plane, span, placed = place(step, source, which == 1)
            sent[span, :] = placed
            spread(step, plane, sent, target.at[core], which, sems.at[zed])
            return carry

        lax.fori_loop(0, PLANES, issue, 0)

    for load in inputs:
        load.wait()

    @pl.when(me > 0)
    def _():
        for copy in before:
            copy.wait_recv()

    @pl.when(me == 0)
    def _():
        prev_in[...] = jnp.zeros_like(prev_in)
        prev_state[...] = jnp.zeros_like(prev_state)

    def recurrence(block, carry):
        at = aligned(block, LANES)
        states = own[0, :, at]
        gate = psend[1, :, at].astype(F32)
        value, back_of = jax.vjp(functools.partial(jax.nn.gelu, approximate=True), gate)
        mixer[:, at] = (states * value).astype(BF)
        gelu[:, at] = value
        slope[:, at] = states * back_of(jnp.ones_like(value))[0]
        shifted[0:8, :] = prev_in[8:16, at].astype(F32)
        shifted[8:, :] = psend[0, :, at].astype(F32)
        conv = taps_ref[0:1, at] * shifted[5 : 5 + tokens, :]
        for tap in range(1, 4):
            conv = conv + taps_ref[tap : tap + 1, at] * shifted[5 + tap : 5 + tap + tokens, :]
        maps = jnp.concatenate([decay_w[block], input_w[block]], axis=1)
        gates = jax.nn.sigmoid(dot_nn(conv.astype(BF), maps))
        recur_gate, input_gate = gates[:, :LANES], gates[:, LANES:]
        rate = -decay_scale * rate_ref[0:1, at]
        log_decay = rate * recur_gate + own[1, :, at]
        decay = jnp.exp(log_decay)
        opening = (iota((tokens, LANES), 0) == 0) & (me == 0)
        mult = jnp.where(opening, 1.0, jnp.sqrt(fallen(-2.0 * log_decay)))
        shifted[0:8, :] = prev_state[:, at]
        shifted[8:, :] = states
        fall = jnp.where(opening, 0.0, input_gate * conv * decay * decay / mult)
        factor = shifted[7 : 7 + tokens, :] * decay - fall
        first[:, at] = factor * rate * recur_gate * (1.0 - recur_gate)
        third_value = mult * input_gate
        second[:, at] = third_value * conv * (1.0 - input_gate)
        third[:, at] = third_value
        decays[block] = decay

        def along(step, carry):
            product, decay = carry
            picked = pl.ds(segment_rows - 1 - step, SEGMENTS, stride=segment_rows)
            product = product * decay
            cumul[block, picked, :] = product
            return product, decays[block, picked, :]

        picked = pl.ds(segment_rows - 1, SEGMENTS, stride=segment_rows)
        decay = decays[block, picked, :]
        product = decay * 0.0 + 1.0
        cumul[block, picked, :] = product
        product, decay = lax.fori_loop(1, segment_rows, along, (product, decay))
        products[:, at] = product * decay
        return carry

    lax.fori_loop(0, blocks, recurrence, 0)

    def share(shift, carry):
        dest = zed * peers + lax.rem(pos + shift, peers)
        remote(
            mixer, plane_ref.at[aligned(pos, tokens)], bulk_sem.at[3], mixer_sem.at[0], sp=dest
        ).start()
        return carry

    lax.fori_loop(1, peers, share, 0)
    keep = pltpu.make_async_copy(mixer, plane_ref.at[aligned(pos, tokens)], mixer_sem.at[1])
    keep.start()

    def from_plane(step):
        return lax.rem(zed + step + 1, PLANES)

    def to_pair(view, slot):
        return remote(view, view, pair_send.at[slot], pair_recv.at[slot], tp=other)

    def pass_rows(step, carry):
        plane = from_plane(step)
        view = rows.at[core, aligned(plane, group)]
        local_wait(view, rows_sem.at[plane])
        to_pair(view, step).start()
        return carry

    lax.fori_loop(0, PLANES, pass_rows, 0)
    for load in loads:
        load.wait()

    def forward(step, carry):
        span = aligned(from_plane(step), group)
        to_pair(rows.at[other, span], step).wait_recv()
        pre[span, :] = dot_nn(rows[0, span, :], wgu[:half, :]) + dot_nn(
            rows[1, span, :], wgu[half:, :]
        )
        return carry

    lax.fori_loop(0, PLANES, forward, 0)
    local_wait(send_r.at[pl.ds(0, (count - 1) * cap)], bulk_sem.at[0])

    def finish(step):
        plane = from_plane(step)
        span = aligned(plane, group)
        to_pair(precv.at[span], 2 * PLANES + step).wait_recv()
        send_r[span, :] = (own[lax.rem(step, 2)] + precv[span, :].astype(F32)).astype(BF)
        spread(step, plane, send_r, back, 2, back_sem.at[zed])

    def swap_part(step, span):
        return remote(
            psend.at[lax.rem(step, 2)], precv.at[span], pair_send.at[2 * PLANES + step],
            pair_recv.at[2 * PLANES + step], tp=other,
        )

    def backward(step, carry):
        plane = from_plane(step)
        span = aligned(plane, group)
        view = grads.at[core, span]
        local_wait(view, grads_sem.at[plane])
        to_pair(view, PLANES + step).start()

        @pl.when(step > 0)
        def _():
            finish(step - 1)

        to_pair(grads.at[other, span], PLANES + step).wait_recv()
        hidden_grad = dot_nt(grads[0, span, :], wd[:, :half]) + dot_nt(
            grads[1, span, :], wd[:, half:]
        )
        gate = pre[span, :hidden]
        up = pre[span, hidden:]
        sig = jax.nn.sigmoid(gate)
        silu = gate * sig
        hid[span, :] = (silu * up).astype(BF)
        xgu[span, :hidden] = (hidden_grad * up * sig * (1.0 + gate * (1.0 - sig))).astype(BF)
        xgu[span, hidden:] = (hidden_grad * silu).astype(BF)

        @pl.when(step > 1)
        def _():
            swap_part(step - 2, span).wait_send()

        psend[lax.rem(step, 2)] = dot_nt(xgu[span, :], wgu[theirs, :]).astype(BF)
        swap_part(step, span).start()
        own[lax.rem(step, 2)] = dot_nt(xgu[span, :], wgu[mine, :])
        return carry

    lax.fori_loop(0, PLANES, backward, 0)
    finish(PLANES - 1)
    out_load = pltpu.make_async_copy(out_w, wgu, load_sem.at[0])
    out_load.start()

    tile = 256

    for side in range(2):
        def weight_tile(step, carry, side=side):
            columns = aligned(step, tile)
            spot = pl.ds(pl.multiple_of(side * half + step * tile, tile), tile)
            both = dot_tn(rows[side, :, columns], xgu[...]).astype(BF)
            gate_g[spot, :] = both[:, :hidden]
            up_g[spot, :] = both[:, hidden:]
            down_g[:, spot] = dot_tn(hid[...], grads[side, :, columns]).astype(BF)
            return carry

        lax.fori_loop(0, half // tile, weight_tile, 0)

    for slot in range(2 * PLANES):
        to_pair(rows.at[0, pl.ds(0, group)], slot).wait_send()
    shared = plane_ref.at[pl.ds(0, (peers - 1) * tokens)]
    local_wait(shared, mixer_sem.at[0])
    keep.wait()
    chunks = peers * tokens // slots
    mixer_loads = [
        pltpu.make_async_copy(
            plane_ref.at[pl.ds(chunk * slots, slots)], rg.at[chunk], load_sem.at[1 + chunk]
        )
        for chunk in range(chunks)
    ]
    for load in mixer_loads:
        load.start()

    def gather(step, carry):
        plane = from_plane(step)
        local_wait(back.at[aligned(plane, group)], back_sem.at[plane])
        return carry

    lax.fori_loop(0, PLANES, gather, 0)
    moe = dot_nn(place_t[...], back[...])
    halves[core] = (moe + cot_ref[:, mine].astype(F32)).astype(BF)
    last = to_pair(halves.at[core], 3 * PLANES)
    last.start()

    cut = width // count
    lane = cols.shape[1] // PLANES
    deep = PLANES // 2

    def column_block(level, place):
        return aligned((level * peers + place) * cut // lane, lane)

    def send_cols(shift, carry):
        place = lax.rem(pos + shift, peers)
        for level in range(deep):
            remote(
                halves.at[core, :, column_block(level, place)],
                cols.at[aligned(pos, tokens), aligned(core * deep + level, lane)],
                bulk_sem.at[4], cols_sem.at[0], sp=zed * peers + place,
            ).start()
        return carry

    lax.fori_loop(1, peers, send_cols, 0)
    kept = [
        pltpu.make_async_copy(
            halves.at[core, :, column_block(level, pos)],
            cols.at[aligned(pos, tokens), aligned(core * deep + level, lane)],
            cols_sem.at[1 + level],
        )
        for level in range(deep)
    ]
    for copy in kept:
        copy.start()

    grad_ref[:, mine] = halves[core]
    out_load.wait()
    to_pair(halves.at[other], 3 * PLANES).wait_recv()
    grad_ref[:, theirs] = halves[other]

    mixer_grad = dot_nn(halves[0], wgu[:half, :]) + dot_nn(halves[1], wgu[half:, :])
    gate_out[...] = (mixer_grad * slope[...]).astype(BF)
    for block in range(blocks):
        at = pl.ds(block * LANES, LANES)
        local[block] = mixer_grad[:, block * LANES : (block + 1) * LANES] * gelu[:, at]

    def scan(step, carry):
        picked = pl.ds(segment_rows - 1 - step, SEGMENTS, stride=segment_rows)
        after = []
        for block in range(blocks):
            total, decay = carry[block]
            total = local[block, picked, :] + decay * total
            local[block, picked, :] = total
            after.append((total, decays[block, picked, :]))
        return after

    picked = pl.ds(segment_rows - 1, SEGMENTS, stride=segment_rows)
    start = [(local[block, picked, :], decays[block, picked, :]) for block in range(blocks)]
    ended = lax.fori_loop(1, segment_rows, scan, start)
    total = jnp.concatenate([piece[0] * piece[1] for piece in ended], axis=1)
    product = products[...]
    whole, entry = product[SEGMENTS - 1 :], total[SEGMENTS - 1 :]
    for segment in range(SEGMENTS - 2, -1, -1):
        row = slice(segment, segment + 1)
        whole = whole * product[row]
        entry = total[row] + product[row] * entry
    pair[0:1, :] = whole
    pair[1:2, :] = entry

    def carry_copy(dest):
        return remote(pair, pieces.at[me], carry_send.at[dest], carry_recv.at[me], sp=dest)

    def send_carry(step, carry):
        carry_copy(me - 1 - step).start()
        return carry

    lax.fori_loop(0, me, send_carry, 0)

    local_wait(cols.at[pl.ds(0, (peers - 1) * tokens), pl.ds(0, deep * lane)], cols_sem.at[0])
    for copy in kept:
        copy.wait()
    cols_mine = cols.at[:, aligned(core, deep * lane)]
    cols_pass = to_pair(cols_mine, 3 * PLANES + 1)
    cols_pass.start()

    def take_carry(step, entering):
        source = count - 1 - step
        local_wait(pieces.at[source], carry_recv.at[source])
        return pieces[source, 0:1, :] * entering + pieces[source, 1:2, :]

    entering = lax.fori_loop(0, count - 1 - me, take_carry, jnp.zeros((1, channels), F32))

    for load in mixer_loads:
        load.wait()
    to_pair(cols.at[:, aligned(other, deep * lane)], 3 * PLANES + 1).wait_recv()
    sums = pl.ds(0, PLANES * lane)
    partial = dot_tn(cols[pl.ds(0, slots), :], rg[0])
    for chunk in range(1, chunks):
        partial = partial + dot_tn(cols[pl.ds(chunk * slots, slots), :], rg[chunk])
    pre[sums, :] = partial
    send_part[...] = partial.astype(BF)

    def part_rows(plane):
        offset = lax.rem((plane * peers + pos) * cut, lane)
        return pl.ds(pl.multiple_of(plane * lane + offset, cut), cut)

    def send_block(shift, carry):
        plane = lax.rem(zed + shift, PLANES)
        remote(
            send_part.at[part_rows(plane)], got_part.at[aligned(zed, cut)],
            bulk_sem.at[5], part_sem.at[zed], sp=plane * peers + pos,
        ).start()
        return carry

    lax.fori_loop(1, PLANES, send_block, 0)

    enter = []
    for segment in range(SEGMENTS - 1, -1, -1):
        enter.append(entering)
        row = slice(segment, segment + 1)
        entering = total[row] + product[row] * entering
    enter = jnp.concatenate(enter[::-1], axis=0)

    for block in range(blocks):
        at = slice(block * LANES, (block + 1) * LANES)
        filled = jnp.broadcast_to(enter[:, None, at], (SEGMENTS, segment_rows, LANES))
        carried = local[block] + cumul[block] * filled.reshape(tokens, LANES)
        both = jnp.concatenate(
            [(carried * first[:, at]).astype(BF), (carried * second[:, at]).astype(BF)], axis=1
        )
        maps = jnp.concatenate([decay_w[block], input_w[block]], axis=1)
        conv_grad[0:tokens, at] = carried * third[:, at] + dot_nt(both, maps)

    halo = pl.ds(tokens, 8)
    halo_copy = remote(
        conv_grad.at[pl.ds(0, 8)], conv_grad.at[halo], halo_sem.at[0], halo_sem.at[1], sp=me - 1
    )

    @pl.when(me > 0)
    def _():
        halo_copy.start()

    @pl.when(me == count - 1)
    def _():
        conv_grad[halo, :] = jnp.zeros((8, channels), F32)

    def taps_over(low, high):
        total = taps_ref[0:1, :] * conv_grad[low + 3 : high + 3, :]
        for tap in range(1, 4):
            total = total + taps_ref[tap : tap + 1, :] * conv_grad[low + 3 - tap : high + 3 - tap, :]
        recur_out[low:high, :] = total.astype(BF)

    taps_over(0, tokens - 16)

    @pl.when(me < count - 1)
    def _():
        local_wait(conv_grad.at[halo], halo_sem.at[1])

    taps_over(tokens - 16, tokens)

    summed = pre[part_rows(zed), :]
    for shift in range(1, PLANES):
        plane = lax.rem(zed + shift, PLANES)
        local_wait(got_part.at[aligned(plane, cut)], part_sem.at[plane])
        summed = summed + got_part[aligned(plane, cut), :].astype(F32)
    weight_out[...] = summed

    local_wait(send_r.at[pl.ds(0, (count - 1) * cap)], bulk_sem.at[1])
    local_wait(send_r.at[pl.ds(0, (count - 1) * cap)], bulk_sem.at[2])
    local_wait(shared, bulk_sem.at[3])
    local_wait(cols.at[pl.ds(0, (peers - 1) * tokens), pl.ds(0, deep * lane)], bulk_sem.at[4])
    local_wait(got_part.at[pl.ds(0, (PLANES - 1) * cut)], bulk_sem.at[5])
    for step in range(PLANES - 2, PLANES):
        swap_part(step, pl.ds(0, group)).wait_send()
    last.wait_send()
    cols_pass.wait_send()

    def sent_carry(step, carry):
        carry_copy(me - 1 - step).wait_send()
        return carry

    lax.fori_loop(0, me, sent_carry, 0)

    @pl.when(me > 0)
    def _():
        halo_copy.wait_send()

    @pl.when(me < count - 1)
    def _():
        for copy in before:
            copy.wait_send()


def flush_kernel(total, *refs):
    sems = refs[-1]
    copies = [
        pltpu.make_async_copy(refs[item], refs[total + item], sems.at[item])
        for item in range(total)
    ]
    for copy in copies:
        copy.start()
    for copy in copies:
        copy.wait()


def flushed(*results):
    total = len(results)
    size = sum(result.size * result.dtype.itemsize for result in results)
    return pl.pallas_call(
        functools.partial(flush_kernel, total),
        in_specs=[pl.BlockSpec(memory_space=pltpu.VMEM)] * total,
        out_specs=[pl.BlockSpec(memory_space=pl.ANY)] * total,
        out_shape=[jax.ShapeDtypeStruct(result.shape, result.dtype) for result in results],
        scratch_shapes=[pltpu.SemaphoreType.DMA((total,))],
        compiler_params=pltpu.CompilerParams(vmem_limit_bytes=4 * 1024 * 1024),
        cost_estimate=pl.CostEstimate(flops=1000, bytes_accessed=2 * size, transcendentals=0),
        name="flush",
    )(*results)


def on_device(
    moe_input,
    cotangent,
    expert_ids,
    route_weight,
    gate_proj,
    up_proj,
    down_proj,
    out_weight,
    recur_input,
    gate_input,
    states,
    conv_taps,
    decay_gate_w,
    input_gate_w,
    decay_rate,
    decay_extra,
):
    count = lax.axis_size("sp")
    tokens, width = moe_input.shape
    cap = max(2, 4 * tokens // count)
    slots = count * cap
    half = width // 2
    hidden = gate_proj.shape[2]
    channels = states.shape[1]
    peers = count // PLANES
    group = peers * cap
    cut = width // count
    lane = max(cut, LANES)
    blocks = channels // LANES
    vmem, anywhere = pl.BlockSpec(memory_space=pltpu.VMEM), pl.BlockSpec(memory_space=pl.ANY)
    dma = pltpu.SemaphoreType.DMA

    def out(shape, kind):
        return jax.ShapeDtypeStruct(shape, kind)

    def plain(kind):
        return pltpu.VMEM((tokens, channels), kind)

    results = pl.pallas_call(
        functools.partial(whole_kernel, count, cap),
        in_specs=[vmem] * 8 + [anywhere] * 8,
        out_specs=[vmem] * 7 + [anywhere],
        out_shape=[
            out((width, hidden), BF), out((width, hidden), BF), out((hidden, width), BF),
            out((cut, channels), F32), out((tokens, width), BF), out((tokens, channels), BF),
            out((tokens, channels), BF), out((peers * tokens, channels), BF),
        ],
        scratch_shapes=[
            pltpu.VMEM((width, 2 * hidden), BF),
            pltpu.VMEM((hidden, width), BF),
            pltpu.VMEM((tokens, slots), BF),
            pltpu.VMEM((tokens, 3 * LANES), BF),
            pltpu.VMEM((slots, half), BF),
            pltpu.VMEM((slots, half), BF),
            pltpu.VMEM((4, slots, half), BF),
            pltpu.VMEM((slots, 2 * hidden), F32),
            pltpu.VMEM((slots, hidden), BF),
            pltpu.VMEM((slots, 2 * hidden), BF),
            pltpu.VMEM((2, group, half), F32),
            pltpu.VMEM((2, group, half), BF),
            pltpu.VMEM((slots, half), BF),
            pltpu.VMEM((slots, half), BF),
            pltpu.VMEM((2, tokens, half), BF),
            plain(BF),
            pltpu.VMEM((peers * tokens, PLANES * lane), BF),
            pltpu.VMEM((PLANES * lane, channels), BF),
            pltpu.VMEM((PLANES * cut, channels), BF),
            plain(F32), plain(F32), plain(F32), plain(F32), plain(F32),
            *[pltpu.VMEM((blocks, tokens, LANES), F32)] * 3,
            pltpu.VMEM((tokens + 8, channels), F32),
            pltpu.VMEM((tokens + 8, LANES), F32),
            pltpu.VMEM((16, channels), BF),
            pltpu.VMEM((8, channels), F32),
            pltpu.VMEM((2, channels), F32),
            pltpu.VMEM((count, 2, channels), F32),
            pltpu.VMEM((SEGMENTS, channels), F32),
            dma((7,)), dma((6,)), dma((PLANES,)), dma((PLANES,)), dma((PLANES,)), dma((2,)),
            dma((3 * PLANES + 2,)), dma((3 * PLANES + 2,)), dma((4,)), dma((3,)), dma((PLANES,)),
            dma((count,)), dma((count,)), dma((2,)),
        ],
        compiler_params=pltpu.CompilerParams(
            collective_id=0, has_side_effects=True, vmem_limit_bytes=62 * 1024 * 1024
        ),
        cost_estimate=pl.CostEstimate(
            flops=16 * slots * width * hidden, bytes_accessed=40 << 20, transcendentals=0
        ),
        name="whole",
    )(
        moe_input, cotangent, expert_ids, route_weight, decay_gate_w, input_gate_w,
        conv_taps.astype(F32), decay_rate[None], gate_proj[0], up_proj[0], down_proj[0], out_weight,
        recur_input, gate_input, states, decay_extra,
    )
    gate_g, up_g, down_g, weight_g, grad, recur_g, gate_in_g = results[:7]
    return (gate_g[None], up_g[None], down_g[None], weight_g, grad, recur_g, gate_in_g)


def solution(mesh):
    return jax.shard_map(
        on_device,
        mesh=mesh,
        in_specs=(
            P("sp", None),
            P("sp", None),
            P("sp", None),
            P("sp", None),
            P("sp", None, "tp"),
            P("sp", None, "tp"),
            P("sp", "tp", None),
            P(None, "tp"),
            P("sp", "tp"),
            P("sp", "tp"),
            P("sp", "tp"),
            P(None, "tp"),
            P("tp", None, None),
            P("tp", None, None),
            P("tp"),
            P("sp", "tp"),
        ),
        out_specs=(
            P("sp", None, "tp"),
            P("sp", None, "tp"),
            P("sp", "tp", None),
            P("sp", "tp"),
            P("sp", None),
            P("sp", "tp"),
            P("sp", "tp"),
        ),
        check_vma=False,
    )
```

time: 255 us -> 214 us (0.84)
  other arithmetic: 17.6 us -> 1.31 us
  local copies, waits for them, and re-layouts: 23 us -> 13.2 us
  Pallas kernels: 204 us -> 198 us
  matrix products: 4.04 us -> 0 us
  starting transfers between devices: 3.4 us -> 0 us
    mul x3 -> x0, other arithmetic: 7.74 us -> none  [the longest x1 5.81 us: on_device(): input_factor = mult * conv * input_gate * (1.0 - input_gate)]
    pallas_call x2 -> x1, Pallas kernels: 204 us -> 198 us  [on_device(): pl.pallas_call(functools.partial(whole_kernel, count, cap), in_specs=[vme...]
    div x2 -> x0, local copies, waits for them, and re-layouts: 5.16 us -> none  [on_device(): recur_gate = jax.nn.sigmoid(decay_pre)]
    unnamed x1 -> x0, other arithmetic: 4.06 us -> none
    dot_general x2 -> x0, matrix products: 4.04 us -> none  [the longest x1 2.57 us: on_device(): jnp.einsum('tbi,bij->tbj', conv_blocks, decay_gate_w, preferred_element_t...]
    reshape x3 -> x0, local copies, waits for them, and re-layouts: 3.81 us -> none  [the longest x2 2.12 us: on_device(): cols = input_grad.reshape(tok_rows, PLANES, peers, width // experts)]
    ppermute x1 -> x0, starting transfers between devices: 3.4 us -> none  [passed_along(): lax.ppermute(value, axis, [(source, source + steps) for source in range(i...]
    unnamed x34 -> x21, local copies, waits for them, and re-layouts: 10.7 us -> 13.2 us
  transfers between devices with their start and end apart: 1 -> 0, of which waited for: 0 -> 0; matrix products, arithmetic and copies ran while one was open for 6% -> 0% of each run, Pallas kernels for 57% -> 0%
where the time goes in v3:
time: 214 us; the launch traced here: 213 us
  Pallas kernels  198 us (93%)
  local copies, waits for them, and re-layouts  13.2 us (6%)
    pallas_call x1, Pallas kernels, on_device(): pl.pallas_call(functools.partial(whole_kernel, count, cap), in_specs=[vme...  198 us
    unnamed x21, local copies, waits for them, and re-layouts  13.2 us

profile of v3, /device:TPU:14, one launch (start us, length us, event | category | flops | bytes accessed | tf_op | source)
XLA Modules:
  0.0 213.4 jit_solution(527600420308495251)
XLA Ops:
  0.6 1.3 convert_element_type.3.taps_ref
  1.9 1.5 copy.23.ids_ref
  3.4 1.5 copy.24.route_ref
  4.9 198.2 %whole.1 = (bf16[2048,512]{1,0:T(8,128)(2,1)}, bf16[2048,512]{1,0:T(8,128)(2,1)}, bf16[512,2048]{1,0:T(8,128)(2,1)}, f32[128,1024]{1,0:T(8,128)}, bf16[256,2048]...) custom-call(bf16[256,2048]{1,0:T(8,128)(2,1)} %tok_ref.1, ...), custom_call_target="tpu_custom_call" | custom-call | flops 17179869184 | bytes 41943040 | tf_op jit(solution)/shard_map/whole/pallas_call | solution.py:630
  203.1 0.0 copy-start.1
  203.1 3.2 %copy.32 = bf16[1,2048,512]{2,1,0:T(8,128)(2,1)} copy(bf16[1,2048,512]{2,1,0:T(8,128)(2,1)} %bitcast.9) | data formatting | bytes 4194304
  206.3 0.0 copy-done.1
  206.3 0.0 copy-start
  206.3 1.3 copy.33
  207.7 1.0 copy-done
  208.7 0.0 copy-start.5
  208.7 0.0 copy-start.2
  208.7 1.3 copy.34
  210.0 0.1 copy-done.5
  210.1 0.0 copy-start.4
  210.1 0.0 copy-start.3
  210.1 0.8 copy.35
  210.9 0.0 copy-done.2
  210.9 1.0 copy.36
  211.8 0.0 copy-done.4
  211.8 0.8 copy.37
  212.6 0.0 copy-done.3
  212.6 0.8 copy.38
Async XLA Ops:
  203.1 3.2 %copy-start.1 = (bf16[2048,512]{1,0:T(8,128)(2,1)S(1)}, bf16[2048,512]{1,0:T(8,128)(2,1)}, u32[]{:S(2)}) copy-start(bf16[2048,512]{1,0:T(8,128)(2,1)} %get-tuple-element.15) | copy-start | bytes 6291460
  206.3 2.3 %copy-start = (bf16[512,2048]{1,0:T(8,128)(2,1)S(1)}, bf16[512,2048]{1,0:T(8,128)(2,1)}, u32[]{:S(2)}) copy-start(bf16[512,2048]{1,0:T(8,128)(2,1)} %get-tuple-element.16) | copy-start | bytes 6291460
  208.7 1.4 copy-start.5
  208.7 2.2 %copy-start.2 = (bf16[256,2048]{1,0:T(8,128)(2,1)S(1)}, bf16[256,2048]{1,0:T(8,128)(2,1)}, u32[]{:S(2)}) copy-start(bf16[256,2048]{1,0:T(8,128)(2,1)} %get-tuple-element.32) | copy-start | bytes 3145732
  210.1 1.8 copy-start.4
  210.1 2.6 %copy-start.3 = (bf16[256,1024]{1,0:T(8,128)(2,1)S(1)}, bf16[256,1024]{1,0:T(8,128)(2,1)}, u32[]{:S(2)}) copy-start(bf16[256,1024]{1,0:T(8,128)(2,1)} %get-tuple-element.34) | copy-start | bytes 1572868

commit v4 on v3

--- a/solution.py
+++ b/solution.py
@@ -58,11 +58,12 @@
     tok_ref, cot_ref, ids_ref, route_ref, decay_w, input_w, taps_ref, rate_ref,
     gate_w, up_w, down_w, out_w, recur_in, gate_in, states_in, extra_in,
     gate_g, up_g, down_g, weight_out, grad_ref, recur_out, gate_out, plane_ref,
-    wgu, wd, place_t, parts, send_r, send_g, rg, pre, hid, xgu, own, psend, precv, back, halves,
-    mixer, cols, send_part, got_part, gelu, slope, first, second, third, decays, cumul, local,
-    conv_grad, shifted, prev_in, prev_state, pair, pieces, products,
+    wgu, wd, table, slot_scale, near_tok, near_cot, far_tok, far_cot, far_ids, far_route, far_moe,
+    send_r, send_g, rg, pre, hid, xgu, own, psend, precv, back, halves,
+    cols, send_part, got_part, gelu, slope, first, second, third, decays, cumul, local,
+    edge, shifted, prev_in, prev_state, pieces, plane_pair, plane_pieces, products,
     load_sem, bulk_sem, rows_sem, grads_sem, back_sem, mixer_sem, pair_send, pair_recv,
-    before_sem, cols_sem, part_sem, carry_send, carry_recv, halo_sem,
+    before_sem, cols_sem, part_sem, carry_recv, plane_send, plane_recv, halo_sem, far_send, far_recv,
 ):
     me, core = lax.axis_index("sp"), lax.axis_index("tp")
     other = 1 - core
@@ -77,6 +78,12 @@
     blocks = channels // LANES
     segment_rows = tokens // SEGMENTS
     mine, theirs = aligned(core, half), aligned(other, half)
+    deep = PLANES // 2
+    base = zed // deep * deep
+    far = lax.rem(zed + deep, PLANES) * peers + pos
+    near_slots = slots // 2
+    conv_grad = own.at[0]
+    mixer = send_part.at[pl.ds(0, tokens)]
     rows, grads = rg.at[pl.ds(0, 2)], rg.at[pl.ds(2, 2)]
 
     loads = [
@@ -90,7 +97,11 @@
         pltpu.make_async_copy(recur_in, psend.at[0], load_sem.at[5]),
         pltpu.make_async_copy(gate_in, psend.at[1], load_sem.at[6]),
     ]
-    for load in inputs + loads:
+    near_loads = [
+        pltpu.make_async_copy(tok_ref.at[:, mine], near_tok, load_sem.at[7]),
+        pltpu.make_async_copy(cot_ref.at[:, mine], near_cot, load_sem.at[8]),
+    ]
+    for load in near_loads + inputs + loads:
         load.start()
 
     barrier = pltpu.get_barrier_semaphore()
@@ -104,25 +115,29 @@
     lax.fori_loop(1, count, greet, 0)
     pl.semaphore_signal(barrier, inc=1, device_id={"tp": other}, device_id_type=MESH)
 
-    ids, route = ids_ref[...], route_ref[...]
-    expert = iota((tokens, LANES), 1)
-    chosen = [ids[:, k : k + 1] == expert for k in range(2)]
-    member = jnp.where(chosen[0] | chosen[1], 1.0, 0.0).astype(BF)
-    earlier = (iota((tokens, tokens), 0) > iota((tokens, tokens), 1)).astype(F32).astype(BF)
-    rank = dot_nn(earlier, member).astype(BF)
-    low = iota((LANES, slots), 0) * cap
-    column = iota((LANES, slots), 1)
-    widen = jnp.where((column >= low) & (column < low + cap), 1.0, 0.0).astype(BF)
-    owner = dot_nn(iota((8, LANES), 1).astype(F32).astype(BF), widen)[0:1]
-    place_in = iota((1, slots), 1).astype(F32) - owner * float(cap)
-    taken = (dot_nn(member, widen) > 0.5) & (dot_nn(rank, widen) == place_in)
-    place_t[...] = jnp.where(taken, 1.0, 0.0).astype(BF)
-    scale = jnp.where(chosen[0], route[:, 0:1], 0.0) + jnp.where(chosen[1], route[:, 1:2], 0.0)
-    for piece in range(3):
-        rounded = scale.astype(BF)
-        parts[:, piece * LANES : (piece + 1) * LANES] = rounded
-        scale = scale - rounded.astype(F32)
-
+    def tabulate(kind, ids, route):
+        expert = iota((LANES, tokens), 0) + base * peers
+        chosen = [ids[k : k + 1, :] == expert for k in range(2)]
+        inside = iota((LANES, tokens), 0) < deep * peers
+        member = jnp.where((chosen[0] | chosen[1]) & inside, 1.0, 0.0).astype(BF)
+        earlier = (iota((tokens, tokens), 0) < iota((tokens, tokens), 1)).astype(F32).astype(BF)
+        rank = dot_nn(member, earlier).astype(BF)
+        low = iota((near_slots, LANES), 1) * cap
+        row = iota((near_slots, LANES), 0)
+        within = (row >= low) & (row < low + cap)
+        widen = jnp.where(within, 1.0, 0.0).astype(BF)
+        place_in = jnp.sum(jnp.where(within, (row - low).astype(F32), 0.0), axis=1, keepdims=True)
+        taken = (dot_nn(widen, member) > 0.5) & (dot_nn(widen, rank) == place_in)
+        table[kind] = jnp.where(taken, 1.0, 0.0).astype(BF)
+        scale = jnp.where(chosen[0], route[0:1, :], 0.0) + jnp.where(chosen[1], route[1:2, :], 0.0)
+        total = jnp.zeros((near_slots, tokens), F32)
+        for _ in range(3):
+            rounded = scale.astype(BF)
+            total = total + dot_nn(widen, rounded)
+            scale = scale - rounded.astype(F32)
+        slot_scale[kind] = jnp.sum(jnp.where(taken, total, 0.0), axis=1, keepdims=True)
+
+    tabulate(0, ids_ref[...], route_ref[...])
     pl.semaphore_wait(barrier, count)
 
     keep_rows = 16
@@ -142,47 +157,63 @@
         for copy in before:
             copy.start()
 
-    def place(step, source, scaled):
-        plane = lax.rem(zed + (PLANES - 1 - step), PLANES)
-        span = aligned(plane, group)
-        chosen_t = place_t[:, span]
-        placed = dot_tn(chosen_t, source[:, mine])
-        if scaled:
-            sums = dot_tn(chosen_t, parts[...])
-            sums = sums[:, :LANES] + sums[:, LANES : 2 * LANES] + sums[:, 2 * LANES :]
-            slot = iota((group, LANES), 0) + plane * group
-            low = iota((group, LANES), 1) * cap
-            own_lane = (slot >= low) & (slot < low + cap)
-            placed = placed * jnp.sum(jnp.where(own_lane, sums, 0.0), axis=1, keepdims=True)
-        return plane, span, placed.astype(BF)
-
-    def spread(step, plane, source, target, which, sem):
+    to_far = [
+        remote(ids_ref, far_ids, far_send.at[0], far_recv.at[0], sp=far),
+        remote(route_ref, far_route, far_send.at[1], far_recv.at[1], sp=far),
+        remote(tok_ref.at[:, mine], far_tok, far_send.at[2], far_recv.at[2], sp=far),
+        remote(cot_ref.at[:, mine], far_cot, far_send.at[3], far_recv.at[3], sp=far),
+    ]
+    for copy in to_far:
+        copy.start()
+
+    def spread(level, source, target, which, sem):
+        plane = base + level
+
         def one(shift, carry):
-            dest = plane * peers + lax.rem(pos + shift, peers)
+            spot = lax.rem(pos + shift, peers)
             remote(
-                source.at[aligned(dest, cap)], target.at[aligned(me, cap)],
-                bulk_sem.at[which], sem, sp=dest,
+                source(plane * peers + spot), target, bulk_sem.at[which], sem,
+                sp=plane * peers + spot,
             ).start()
             return carry
 
-        lax.fori_loop(jnp.where(step == PLANES - 1, 1, 0), peers, one, 0)
-
-        @pl.when(step == PLANES - 1)
+        here = plane == zed
+        lax.fori_loop(jnp.where(here, 1, 0), peers, one, 0)
+
+        @pl.when(here)
         def _():
-            pltpu.make_async_copy(
-                source.at[aligned(me, cap)], target.at[aligned(me, cap)], sem
-            ).start()
-
-    for which, (source, sent, target, sems) in enumerate(
-        ((tok_ref, send_r, rows, rows_sem), (cot_ref, send_g, grads, grads_sem))
-    ):
-        def issue(step, carry, which=which, source=source, sent=sent, target=target, sems=sems):
-            plane, span, placed = place(step, source, which == 1)
-            sent[span, :] = placed
-            spread(step, plane, sent, target.at[core], which, sems.at[zed])
+            pltpu.make_async_copy(source(me), target, sem).start()
+
+    def dispatch(kind, which):
+        tokens_in = (
+            (near_tok, near_cot) if kind == 0 else (far_tok, far_cot)
+        )[which]
+        sent = (send_r, send_g)[which]
+        target = (rows, grads)[which]
+        sems = (rows_sem, grads_sem)[which]
+        origin = me if kind == 0 else far
+        plane_of = zed if kind == 0 else lax.rem(zed + deep, PLANES)
+
+        def issue(step, carry):
+            level = lax.rem(zed - base + 1 + step, deep)
+            span = aligned(level, group)
+            placed = dot_nn(table[kind, span, :], tokens_in[...])
+            if which == 1:
+                placed = placed * slot_scale[kind, span, :]
+            sent[kind, span, :] = placed.astype(BF)
+            spread(
+                level,
+                lambda dest: sent.at[kind, aligned(dest - base * peers, cap)],
+                target.at[core, aligned(origin, cap)], which, sems.at[plane_of],
+            )
             return carry
 
-        lax.fori_loop(0, PLANES, issue, 0)
+        lax.fori_loop(0, deep, issue, 0)
+
+    near_loads[0].wait()
+    dispatch(0, 0)
+    near_loads[1].wait()
+    dispatch(0, 1)
 
     for load in inputs:
         load.wait()
@@ -256,8 +287,14 @@
     keep = pltpu.make_async_copy(mixer, plane_ref.at[aligned(pos, tokens)], mixer_sem.at[1])
     keep.start()
 
+    to_far[0].wait_recv()
+    to_far[1].wait_recv()
+    tabulate(1, far_ids[...], far_route[...])
+    to_far[2].wait_recv()
+    dispatch(1, 0)
+
     def from_plane(step):
-        return lax.rem(zed + step + 1, PLANES)
+        return lax.rem(base + deep * (step // deep) + lax.rem(zed - base + step, deep), PLANES)
 
     def to_pair(view, slot):
         return remote(view, view, pair_send.at[slot], pair_recv.at[slot], tp=other)
@@ -269,7 +306,7 @@
         to_pair(view, step).start()
         return carry
 
-    lax.fori_loop(0, PLANES, pass_rows, 0)
+    lax.fori_loop(0, deep, pass_rows, 0)
     for load in loads:
         load.wait()
 
@@ -281,15 +318,27 @@
         )
         return carry
 
-    lax.fori_loop(0, PLANES, forward, 0)
-    local_wait(send_r.at[pl.ds(0, (count - 1) * cap)], bulk_sem.at[0])
+    lax.fori_loop(0, deep, forward, 0)
+    to_far[3].wait_recv()
+    dispatch(1, 1)
+    lax.fori_loop(deep, PLANES, pass_rows, 0)
+    lax.fori_loop(deep, PLANES, forward, 0)
+    sent_bytes = precv.at[pl.ds(0, 2 * (deep * peers - 1) * cap)]
+    local_wait(sent_bytes, bulk_sem.at[0])
 
     def finish(step):
         plane = from_plane(step)
         span = aligned(plane, group)
         to_pair(precv.at[span], 2 * PLANES + step).wait_recv()
-        send_r[span, :] = (own[lax.rem(step, 2)] + precv[span, :].astype(F32)).astype(BF)
-        spread(step, plane, send_r, back, 2, back_sem.at[zed])
+        kind = step // deep
+        level = lax.rem(plane, deep)
+        near = aligned(level, group)
+        send_r[kind, near, :] = (own[lax.rem(step, 2)] + precv[span, :].astype(F32)).astype(BF)
+        spread(
+            level,
+            lambda dest: send_r.at[kind, aligned(dest - base * peers, cap)],
+            back.at[kind, aligned(me - base * peers, cap)], 2, back_sem.at[kind * deep + zed - base],
+        )
 
     def swap_part(step, span):
         return remote(
@@ -336,8 +385,8 @@
 
     tile = 256
 
-    for side in range(2):
-        def weight_tile(step, carry, side=side):
+    def weigh(side):
+        def weight_tile(step, carry):
             columns = aligned(step, tile)
             spot = pl.ds(pl.multiple_of(side * half + step * tile, tile), tile)
             both = dot_tn(rows[side, :, columns], xgu[...]).astype(BF)
@@ -348,11 +397,24 @@
 
         lax.fori_loop(0, half // tile, weight_tile, 0)
 
+    weigh(0)
+
+    def gather(step, carry):
+        kind, level = step // deep, lax.rem(step, deep)
+        local_wait(back.at[kind, aligned(level, group)], back_sem.at[step])
+        return carry
+
+    lax.fori_loop(deep, PLANES, gather, 0)
+    far_tok[...] = dot_tn(table[1], back[1]).astype(BF)
+    far_sum = remote(far_tok, far_moe, far_send.at[4], far_recv.at[4], sp=far)
+    far_sum.start()
+    weigh(1)
     for slot in range(2 * PLANES):
         to_pair(rows.at[0, pl.ds(0, group)], slot).wait_send()
     shared = plane_ref.at[pl.ds(0, (peers - 1) * tokens)]
     local_wait(shared, mixer_sem.at[0])
     keep.wait()
+    local_wait(shared, bulk_sem.at[3])
     chunks = peers * tokens // slots
     mixer_loads = [
         pltpu.make_async_copy(
@@ -363,20 +425,15 @@
     for load in mixer_loads:
         load.start()
 
-    def gather(step, carry):
-        plane = from_plane(step)
-        local_wait(back.at[aligned(plane, group)], back_sem.at[plane])
-        return carry
-
-    lax.fori_loop(0, PLANES, gather, 0)
-    moe = dot_nn(place_t[...], back[...])
-    halves[core] = (moe + cot_ref[:, mine].astype(F32)).astype(BF)
+    lax.fori_loop(0, deep, gather, 0)
+    moe = dot_tn(table[0], back[0]) + near_cot[...].astype(F32)
+    far_sum.wait_recv()
+    halves[core] = (moe + far_moe[...].astype(F32)).astype(BF)
     last = to_pair(halves.at[core], 3 * PLANES)
     last.start()
 
     cut = width // count
     lane = cols.shape[1] // PLANES
-    deep = PLANES // 2
 
     def column_block(level, place):
         return aligned((level * peers + place) * cut // lane, lane)
@@ -434,17 +491,46 @@
         row = slice(segment, segment + 1)
         whole = whole * product[row]
         entry = total[row] + product[row] * entry
-    pair[0:1, :] = whole
-    pair[1:2, :] = entry
-
-    def carry_copy(dest):
-        return remote(pair, pieces.at[me], carry_send.at[dest], carry_recv.at[me], sp=dest)
-
-    def send_carry(step, carry):
-        carry_copy(me - 1 - step).start()
-        return carry
-
-    lax.fori_loop(0, me, send_carry, 0)
+    pieces[pos, 0:1, :] = whole
+    pieces[pos, 1:2, :] = entry
+
+    def send_carry(shift, carry):
+        dest = zed * peers + lax.rem(pos + shift, peers)
+        remote(pieces.at[pos], pieces.at[pos], bulk_sem.at[6], carry_recv.at[pos], sp=dest).start()
+        return carry
+
+    lax.fori_loop(1, peers, send_carry, 0)
+
+    def wait_carry(shift, carry):
+        source = lax.rem(pos + shift, peers)
+        local_wait(pieces.at[source], carry_recv.at[source])
+        return carry
+
+    lax.fori_loop(1, peers, wait_carry, 0)
+    blank = whole * 0.0
+    whole, entry = blank + 1.0, blank
+    after, after_entry = whole, entry
+    for spot in range(peers - 1, -1, -1):
+        factor, addend = pieces[spot, 0:1, :], pieces[spot, 1:2, :]
+        whole = factor * whole
+        entry = addend + factor * entry
+        later = spot > pos
+        after = jnp.where(later, factor * after, after)
+        after_entry = jnp.where(later, addend + factor * after_entry, after_entry)
+    plane_pair[0:1, :] = whole
+    plane_pair[1:2, :] = entry
+
+    def plane_copy(plane):
+        return remote(
+            plane_pair, plane_pieces.at[zed], plane_send.at[plane], plane_recv.at[zed],
+            sp=plane * peers + pos,
+        )
+
+    def send_plane(step, carry):
+        plane_copy(zed - 1 - step).start()
+        return carry
+
+    lax.fori_loop(0, zed, send_plane, 0)
 
     local_wait(cols.at[pl.ds(0, (peers - 1) * tokens), pl.ds(0, deep * lane)], cols_sem.at[0])
     for copy in kept:
@@ -452,13 +538,6 @@
     cols_mine = cols.at[:, aligned(core, deep * lane)]
     cols_pass = to_pair(cols_mine, 3 * PLANES + 1)
     cols_pass.start()
-
-    def take_carry(step, entering):
-        source = count - 1 - step
-        local_wait(pieces.at[source], carry_recv.at[source])
-        return pieces[source, 0:1, :] * entering + pieces[source, 1:2, :]
-
-    entering = lax.fori_loop(0, count - 1 - me, take_carry, jnp.zeros((1, channels), F32))
 
     for load in mixer_loads:
         load.wait()
@@ -484,6 +563,13 @@
 
     lax.fori_loop(1, PLANES, send_block, 0)
 
+    def take_plane(step, entering):
+        source = PLANES - 1 - step
+        local_wait(plane_pieces.at[source], plane_recv.at[source])
+        return plane_pieces[source, 0:1, :] * entering + plane_pieces[source, 1:2, :]
+
+    entering = lax.fori_loop(0, PLANES - 1 - zed, take_plane, blank)
+    entering = after_entry + after * entering
     enter = []
     for segment in range(SEGMENTS - 1, -1, -1):
         enter.append(entering)
@@ -501,9 +587,9 @@
         maps = jnp.concatenate([decay_w[block], input_w[block]], axis=1)
         conv_grad[0:tokens, at] = carried * third[:, at] + dot_nt(both, maps)
 
-    halo = pl.ds(tokens, 8)
+    halo = pl.ds(16, 8)
     halo_copy = remote(
-        conv_grad.at[pl.ds(0, 8)], conv_grad.at[halo], halo_sem.at[0], halo_sem.at[1], sp=me - 1
+        conv_grad.at[pl.ds(0, 8)], edge.at[halo], halo_sem.at[0], halo_sem.at[1], sp=me - 1
     )
 
     @pl.when(me > 0)
@@ -512,21 +598,23 @@
 
     @pl.when(me == count - 1)
     def _():
-        conv_grad[halo, :] = jnp.zeros((8, channels), F32)
-
-    def taps_over(low, high):
-        total = taps_ref[0:1, :] * conv_grad[low + 3 : high + 3, :]
+        edge[halo, :] = jnp.zeros((8, channels), F32)
+
+    edge[0:16, :] = conv_grad[tokens - 16 : tokens, :]
+
+    def taps_over(source, rows):
+        total = taps_ref[0:1, :] * source[3 : rows + 3, :]
         for tap in range(1, 4):
-            total = total + taps_ref[tap : tap + 1, :] * conv_grad[low + 3 - tap : high + 3 - tap, :]
-        recur_out[low:high, :] = total.astype(BF)
-
-    taps_over(0, tokens - 16)
+            total = total + taps_ref[tap : tap + 1, :] * source[3 - tap : rows + 3 - tap, :]
+        return total.astype(BF)
+
+    recur_out[0 : tokens - 16, :] = taps_over(conv_grad, tokens - 16)
 
     @pl.when(me < count - 1)
     def _():
-        local_wait(conv_grad.at[halo], halo_sem.at[1])
-
-    taps_over(tokens - 16, tokens)
+        local_wait(edge.at[halo], halo_sem.at[1])
+
+    recur_out[tokens - 16 : tokens, :] = taps_over(edge, 16)
 
     summed = pre[part_rows(zed), :]
     for shift in range(1, PLANES):
@@ -535,9 +623,12 @@
         summed = summed + got_part[aligned(plane, cut), :].astype(F32)
     weight_out[...] = summed
 
-    local_wait(send_r.at[pl.ds(0, (count - 1) * cap)], bulk_sem.at[1])
-    local_wait(send_r.at[pl.ds(0, (count - 1) * cap)], bulk_sem.at[2])
-    local_wait(shared, bulk_sem.at[3])
+    for which in (1, 2):
+        local_wait(sent_bytes, bulk_sem.at[which])
+    local_wait(pieces.at[pl.ds(0, peers - 1)], bulk_sem.at[6])
+    for copy in to_far:
+        copy.wait_send()
+    far_sum.wait_send()
     local_wait(cols.at[pl.ds(0, (peers - 1) * tokens), pl.ds(0, deep * lane)], bulk_sem.at[4])
     local_wait(got_part.at[pl.ds(0, (PLANES - 1) * cut)], bulk_sem.at[5])
     for step in range(PLANES - 2, PLANES):
@@ -545,11 +636,11 @@
     last.wait_send()
     cols_pass.wait_send()
 
-    def sent_carry(step, carry):
-        carry_copy(me - 1 - step).wait_send()
-        return carry
-
-    lax.fori_loop(0, me, sent_carry, 0)
+    def sent_plane(step, carry):
+        plane_copy(zed - 1 - step).wait_send()
+        return carry
+
+    lax.fori_loop(0, zed, sent_plane, 0)
 
     @pl.when(me > 0)
     def _():
@@ -622,27 +713,34 @@
     dma = pltpu.SemaphoreType.DMA
 
     def out(shape, kind):
-        return jax.ShapeDtypeStruct(shape, kind)
+        return pltpu.VMEM(shape, kind)
 
     def plain(kind):
         return pltpu.VMEM((tokens, channels), kind)
 
     results = pl.pallas_call(
         functools.partial(whole_kernel, count, cap),
-        in_specs=[vmem] * 8 + [anywhere] * 8,
+        in_specs=[anywhere] * 2 + [vmem] * 6 + [anywhere] * 8,
         out_specs=[vmem] * 7 + [anywhere],
         out_shape=[
             out((width, hidden), BF), out((width, hidden), BF), out((hidden, width), BF),
             out((cut, channels), F32), out((tokens, width), BF), out((tokens, channels), BF),
-            out((tokens, channels), BF), out((peers * tokens, channels), BF),
+            out((tokens, channels), BF), jax.ShapeDtypeStruct((peers * tokens, channels), BF),
         ],
         scratch_shapes=[
             pltpu.VMEM((width, 2 * hidden), BF),
             pltpu.VMEM((hidden, width), BF),
-            pltpu.VMEM((tokens, slots), BF),
-            pltpu.VMEM((tokens, 3 * LANES), BF),
-            pltpu.VMEM((slots, half), BF),
-            pltpu.VMEM((slots, half), BF),
+            pltpu.VMEM((2, slots // 2, tokens), BF),
+            pltpu.VMEM((2, slots // 2, 1), F32),
+            pltpu.VMEM((tokens, half), BF),
+            pltpu.VMEM((tokens, half), BF),
+            pltpu.VMEM((tokens, half), BF),
+            pltpu.VMEM((tokens, half), BF),
+            pltpu.VMEM((2, tokens), jnp.int32),
+            pltpu.VMEM((2, tokens), F32),
+            pltpu.VMEM((tokens, half), BF),
+            pltpu.VMEM((2, slots // 2, half), BF),
+            pltpu.VMEM((2, slots // 2, half), BF),
             pltpu.VMEM((4, slots, half), BF),
             pltpu.VMEM((slots, 2 * hidden), F32),
             pltpu.VMEM((slots, hidden), BF),
@@ -650,38 +748,38 @@
             pltpu.VMEM((2, group, half), F32),
             pltpu.VMEM((2, group, half), BF),
             pltpu.VMEM((slots, half), BF),
-            pltpu.VMEM((slots, half), BF),
+            pltpu.VMEM((2, slots // 2, half), BF),
             pltpu.VMEM((2, tokens, half), BF),
-            plain(BF),
             pltpu.VMEM((peers * tokens, PLANES * lane), BF),
             pltpu.VMEM((PLANES * lane, channels), BF),
             pltpu.VMEM((PLANES * cut, channels), BF),
             plain(F32), plain(F32), plain(F32), plain(F32), plain(F32),
             *[pltpu.VMEM((blocks, tokens, LANES), F32)] * 3,
-            pltpu.VMEM((tokens + 8, channels), F32),
+            pltpu.VMEM((24, channels), F32),
             pltpu.VMEM((tokens + 8, LANES), F32),
             pltpu.VMEM((16, channels), BF),
             pltpu.VMEM((8, channels), F32),
+            pltpu.VMEM((peers, 2, channels), F32),
             pltpu.VMEM((2, channels), F32),
-            pltpu.VMEM((count, 2, channels), F32),
+            pltpu.VMEM((PLANES, 2, channels), F32),
             pltpu.VMEM((SEGMENTS, channels), F32),
-            dma((7,)), dma((6,)), dma((PLANES,)), dma((PLANES,)), dma((PLANES,)), dma((2,)),
+            dma((9,)), dma((7,)), dma((PLANES,)), dma((PLANES,)), dma((PLANES,)), dma((2,)),
             dma((3 * PLANES + 2,)), dma((3 * PLANES + 2,)), dma((4,)), dma((3,)), dma((PLANES,)),
-            dma((count,)), dma((count,)), dma((2,)),
+            dma((peers,)), dma((PLANES,)), dma((PLANES,)), dma((2,)), dma((5,)), dma((5,)),
         ],
         compiler_params=pltpu.CompilerParams(
-            collective_id=0, has_side_effects=True, vmem_limit_bytes=62 * 1024 * 1024
+            collective_id=0, has_side_effects=True, vmem_limit_bytes=54 * 1024 * 1024
         ),
         cost_estimate=pl.CostEstimate(
             flops=16 * slots * width * hidden, bytes_accessed=40 << 20, transcendentals=0
         ),
         name="whole",
     )(
-        moe_input, cotangent, expert_ids, route_weight, decay_gate_w, input_gate_w,
+        moe_input, cotangent, expert_ids.T, route_weight.T, decay_gate_w, input_gate_w,
         conv_taps.astype(F32), decay_rate[None], gate_proj[0], up_proj[0], down_proj[0], out_weight,
         recur_input, gate_input, states, decay_extra,
     )
-    gate_g, up_g, down_g, weight_g, grad, recur_g, gate_in_g = results[:7]
+    gate_g, up_g, down_g, weight_g, grad, recur_g, gate_in_g = flushed(*results[:7])
     return (gate_g[None], up_g[None], down_g[None], weight_g, grad, recur_g, gate_in_g)
 
 

time: 214 us -> 171 us (0.80)
  Pallas kernels: 198 us -> 169 us
  local copies, waits for them, and re-layouts: 13.2 us -> 0 us
    pallas_call x1 -> x2, Pallas kernels: 198 us -> 169 us  [the longest x1 165 us: on_device(): pl.pallas_call(functools.partial(whole_kernel, count, cap), in_specs=[any...]
    unnamed x21 -> x0, local copies, waits for them, and re-layouts: 13.2 us -> none
where the time goes in v4:
time: 171 us; the launch traced here: 170 us
  Pallas kernels  169 us (99%)
    pallas_call x1, Pallas kernels, on_device(): pl.pallas_call(functools.partial(whole_kernel, count, cap), in_specs=[any...  165 us
    pallas_call x1, Pallas kernels, flushed(): pl.pallas_call(functools.partial(flush_kernel, total), in_specs=[pl.Block...  3.5 us

profile of v4, /device:TPU:14, one launch (start us, length us, event | category | flops | bytes accessed | tf_op | source)
XLA Modules:
  0.0 170.5 jit_solution(12088496572342093031)
XLA Ops:
  0.6 1.3 convert_element_type.3.taps_ref
  1.9 165.0 %whole.1 = (bf16[2048,512]{1,0:T(8,128)(2,1)S(1)}, bf16[2048,512]{1,0:T(8,128)(2,1)S(1)}, bf16[512,2048]{1,0:T(8,128)(2,1)S(1)}, f32[128,1024]{1,0:T(8,128)S(1)}...) custom-call(bf16[256,2048]{1,0:T(8,128)(2,1)} %tok_ref.1, ...), custom_call_target="tpu_custom_call" | custom-call | flops 17179869184 | bytes 41943040 | tf_op jit(solution)/shard_map/whole/pallas_call | solution.py:721
  167.0 3.5 %flush.1 = (bf16[2048,512]{1,0:T(8,128)(2,1)}, bf16[2048,512]{1,0:T(8,128)(2,1)}, bf16[512,2048]{1,0:T(8,128)(2,1)}, f32[128,1024]{1,0:T(8,128)}, bf16[256,2048]...) custom-call(bf16[2048,512]{1,0:T(8,128)(2,1)S(1)} %get-tuple-element.21.refs_0_, ...), custom_call_target="tpu_custom_call" | custom-call | flops 1000 | bytes 17825792 | tf_op jit(solution)/shard_map/flush/pallas_call | solution.py:670

commit v5 on v4

--- a/solution.py
+++ b/solution.py
@@ -55,13 +55,13 @@
 
 def whole_kernel(
     count, cap,
-    tok_ref, cot_ref, ids_ref, route_ref, decay_w, input_w, taps_ref, rate_ref,
+    tok_ref, cot_ref, ids_ref, route_ref, decay_w, input_w, taps_in, rate_ref,
     gate_w, up_w, down_w, out_w, recur_in, gate_in, states_in, extra_in,
     gate_g, up_g, down_g, weight_out, grad_ref, recur_out, gate_out, plane_ref,
     wgu, wd, table, slot_scale, near_tok, near_cot, far_tok, far_cot, far_ids, far_route, far_moe,
     send_r, send_g, rg, pre, hid, xgu, own, psend, precv, back, halves,
     cols, send_part, got_part, gelu, slope, first, second, third, decays, cumul, local,
-    edge, shifted, prev_in, prev_state, pieces, plane_pair, plane_pieces, products,
+    taps_ref, edge, shifted, prev_in, prev_state, pieces, plane_pair, plane_pieces, products,
     load_sem, bulk_sem, rows_sem, grads_sem, back_sem, mixer_sem, pair_send, pair_recv,
     before_sem, cols_sem, part_sem, carry_recv, plane_send, plane_recv, halo_sem, far_send, far_recv,
 ):
@@ -137,6 +137,7 @@
             scale = scale - rounded.astype(F32)
         slot_scale[kind] = jnp.sum(jnp.where(taken, total, 0.0), axis=1, keepdims=True)
 
+    taps_ref[...] = taps_in[...].astype(F32)
     tabulate(0, ids_ref[...], route_ref[...])
     pl.semaphore_wait(barrier, count)
 
@@ -204,7 +205,7 @@
             spread(
                 level,
                 lambda dest: sent.at[kind, aligned(dest - base * peers, cap)],
-                target.at[core, aligned(origin, cap)], which, sems.at[plane_of],
+                target.at[core, aligned(origin, cap)], which + 7 * kind * (1 - which), sems.at[plane_of],
             )
             return carry
 
@@ -276,17 +277,6 @@
 
     lax.fori_loop(0, blocks, recurrence, 0)
 
-    def share(shift, carry):
-        dest = zed * peers + lax.rem(pos + shift, peers)
-        remote(
-            mixer, plane_ref.at[aligned(pos, tokens)], bulk_sem.at[3], mixer_sem.at[0], sp=dest
-        ).start()
-        return carry
-
-    lax.fori_loop(1, peers, share, 0)
-    keep = pltpu.make_async_copy(mixer, plane_ref.at[aligned(pos, tokens)], mixer_sem.at[1])
-    keep.start()
-
     to_far[0].wait_recv()
     to_far[1].wait_recv()
     tabulate(1, far_ids[...], far_route[...])
@@ -321,10 +311,9 @@
     lax.fori_loop(0, deep, forward, 0)
     to_far[3].wait_recv()
     dispatch(1, 1)
-    lax.fori_loop(deep, PLANES, pass_rows, 0)
-    lax.fori_loop(deep, PLANES, forward, 0)
+    near_bytes = precv.at[pl.ds(0, (deep * peers - 1) * cap)]
     sent_bytes = precv.at[pl.ds(0, 2 * (deep * peers - 1) * cap)]
-    local_wait(sent_bytes, bulk_sem.at[0])
+    local_wait(near_bytes, bulk_sem.at[0])
 
     def finish(step):
         plane = from_plane(step)
@@ -334,6 +323,9 @@
         level = lax.rem(plane, deep)
         near = aligned(level, group)
         send_r[kind, near, :] = (own[lax.rem(step, 2)] + precv[span, :].astype(F32)).astype(BF)
+
+    def release(step):
+        kind, level = step // deep, lax.rem(from_plane(step), deep)
         spread(
             level,
             lambda dest: send_r.at[kind, aligned(dest - base * peers, cap)],
@@ -346,16 +338,18 @@
             pair_recv.at[2 * PLANES + step], tp=other,
         )
 
-    def backward(step, carry):
+    def backward(step, eager):
         plane = from_plane(step)
         span = aligned(plane, group)
         view = grads.at[core, span]
         local_wait(view, grads_sem.at[plane])
         to_pair(view, PLANES + step).start()
 
-        @pl.when(step > 0)
+        @pl.when(lax.rem(step, deep) > 0)
         def _():
             finish(step - 1)
+            if eager:
+                release(step - 1)
 
         to_pair(grads.at[other, span], PLANES + step).wait_recv()
         hidden_grad = dot_nt(grads[0, span, :], wd[:, :half]) + dot_nt(
@@ -376,10 +370,40 @@
         psend[lax.rem(step, 2)] = dot_nt(xgu[span, :], wgu[theirs, :]).astype(BF)
         swap_part(step, span).start()
         own[lax.rem(step, 2)] = dot_nt(xgu[span, :], wgu[mine, :])
-        return carry
-
-    lax.fori_loop(0, PLANES, backward, 0)
+
+    def quiet_backward(step, carry):
+        backward(step, False)
+        return carry
+
+    def eager_backward(step, carry):
+        backward(step, True)
+        return carry
+
+    def late_release(step, carry):
+        release(step)
+        return carry
+
+    lax.fori_loop(0, deep, quiet_backward, 0)
+    finish(deep - 1)
+    lax.fori_loop(deep, PLANES, pass_rows, 0)
+    lax.fori_loop(deep, PLANES, forward, 0)
+    local_wait(near_bytes, bulk_sem.at[7])
+    lax.fori_loop(deep, PLANES, eager_backward, 0)
     finish(PLANES - 1)
+    release(PLANES - 1)
+    lax.fori_loop(0, deep, late_release, 0)
+
+    def share(shift, carry):
+        dest = zed * peers + lax.rem(pos + shift, peers)
+        remote(
+            mixer, plane_ref.at[aligned(pos, tokens)], bulk_sem.at[3], mixer_sem.at[0], sp=dest
+        ).start()
+        return carry
+
+    lax.fori_loop(1, peers, share, 0)
+    keep = pltpu.make_async_copy(mixer, plane_ref.at[aligned(pos, tokens)], mixer_sem.at[1])
+    keep.start()
+
     out_load = pltpu.make_async_copy(out_w, wgu, load_sem.at[0])
     out_load.start()
 
@@ -755,6 +779,7 @@
             pltpu.VMEM((PLANES * cut, channels), BF),
             plain(F32), plain(F32), plain(F32), plain(F32), plain(F32),
             *[pltpu.VMEM((blocks, tokens, LANES), F32)] * 3,
+            pltpu.VMEM((4, channels), F32),
             pltpu.VMEM((24, channels), F32),
             pltpu.VMEM((tokens + 8, LANES), F32),
             pltpu.VMEM((16, channels), BF),
@@ -763,7 +788,7 @@
             pltpu.VMEM((2, channels), F32),
             pltpu.VMEM((PLANES, 2, channels), F32),
             pltpu.VMEM((SEGMENTS, channels), F32),
-            dma((9,)), dma((7,)), dma((PLANES,)), dma((PLANES,)), dma((PLANES,)), dma((2,)),
+            dma((9,)), dma((8,)), dma((PLANES,)), dma((PLANES,)), dma((PLANES,)), dma((2,)),
             dma((3 * PLANES + 2,)), dma((3 * PLANES + 2,)), dma((4,)), dma((3,)), dma((PLANES,)),
             dma((peers,)), dma((PLANES,)), dma((PLANES,)), dma((2,)), dma((5,)), dma((5,)),
         ],
@@ -776,7 +801,7 @@
         name="whole",
     )(
         moe_input, cotangent, expert_ids.T, route_weight.T, decay_gate_w, input_gate_w,
-        conv_taps.astype(F32), decay_rate[None], gate_proj[0], up_proj[0], down_proj[0], out_weight,
+        conv_taps, decay_rate[None], gate_proj[0], up_proj[0], down_proj[0], out_weight,
         recur_input, gate_input, states, decay_extra,
     )
     gate_g, up_g, down_g, weight_g, grad, recur_g, gate_in_g = flushed(*results[:7])

time: 171 us -> 165 us (0.965)
  Pallas kernels: 169 us -> 164 us
    pallas_call x1, Pallas kernels: 165 us -> 160 us  [on_device(): pl.pallas_call(functools.partial(whole_kernel, count, cap), in_specs=[any...]
where the time goes in v5:
time: 165 us
  Pallas kernels  164 us (99%)
    pallas_call x1, Pallas kernels, on_device(): pl.pallas_call(functools.partial(whole_kernel, count, cap), in_specs=[any...  160 us
    pallas_call x1, Pallas kernels, flushed(): pl.pallas_call(functools.partial(flush_kernel, total), in_specs=[pl.Block...  3.5 us

profile of v5, /device:TPU:14, one launch (start us, length us, event | category | flops | bytes accessed | tf_op | source)
XLA Modules:
  0.0 164.6 jit_solution(13549108850025448128)
XLA Ops:
  0.6 160.3 %whole.1 = (bf16[2048,512]{1,0:T(8,128)(2,1)S(1)}, bf16[2048,512]{1,0:T(8,128)(2,1)S(1)}, bf16[512,2048]{1,0:T(8,128)(2,1)S(1)}, f32[128,1024]{1,0:T(8,128)S(1)}...) custom-call(bf16[256,2048]{1,0:T(8,128)(2,1)} %tok_ref.1, ...), custom_call_target="tpu_custom_call" | custom-call | flops 17179869184 | bytes 41943040 | tf_op jit(solution)/shard_map/whole/pallas_call | solution.py:745
  160.9 3.5 %flush.1 = (bf16[2048,512]{1,0:T(8,128)(2,1)}, bf16[2048,512]{1,0:T(8,128)(2,1)}, bf16[512,2048]{1,0:T(8,128)(2,1)}, f32[128,1024]{1,0:T(8,128)}, bf16[256,2048]...) custom-call(bf16[2048,512]{1,0:T(8,128)(2,1)S(1)} %get-tuple-element.21.refs_0_, ...), custom_call_target="tpu_custom_call" | custom-call | flops 1000 | bytes 17825792 | tf_op jit(solution)/shard_map/flush/pallas_call | solution.py:694

commit v6 on v5

--- a/solution.py
+++ b/solution.py
@@ -525,6 +525,13 @@
 
     lax.fori_loop(1, peers, send_carry, 0)
 
+    local_wait(cols.at[pl.ds(0, (peers - 1) * tokens), pl.ds(0, deep * lane)], cols_sem.at[0])
+    for copy in kept:
+        copy.wait()
+    cols_mine = cols.at[:, aligned(core, deep * lane)]
+    cols_pass = to_pair(cols_mine, 3 * PLANES + 1)
+    cols_pass.start()
+
     def wait_carry(shift, carry):
         source = lax.rem(pos + shift, peers)
         local_wait(pieces.at[source], carry_recv.at[source])
@@ -555,13 +562,6 @@
         return carry
 
     lax.fori_loop(0, zed, send_plane, 0)
-
-    local_wait(cols.at[pl.ds(0, (peers - 1) * tokens), pl.ds(0, deep * lane)], cols_sem.at[0])
-    for copy in kept:
-        copy.wait()
-    cols_mine = cols.at[:, aligned(core, deep * lane)]
-    cols_pass = to_pair(cols_mine, 3 * PLANES + 1)
-    cols_pass.start()
 
     for load in mixer_loads:
         load.wait()

time: 165 us -> 164 us (level)
  no operation moved by 1% of the time
where the time goes in v6:
time: 164 us; the launch traced here: 163 us
  Pallas kernels  163 us (99%)
    pallas_call x1, Pallas kernels, on_device(): pl.pallas_call(functools.partial(whole_kernel, count, cap), in_specs=[any...  159 us
    pallas_call x1, Pallas kernels, flushed(): pl.pallas_call(functools.partial(flush_kernel, total), in_specs=[pl.Block...  3.5 us

profile of v6, /device:TPU:14, one launch (start us, length us, event | category | flops | bytes accessed | tf_op | source)
XLA Modules:
  0.0 163.4 jit_solution(17345442314534272937)
XLA Ops:
  0.6 159.1 %whole.1 = (bf16[2048,512]{1,0:T(8,128)(2,1)S(1)}, bf16[2048,512]{1,0:T(8,128)(2,1)S(1)}, bf16[512,2048]{1,0:T(8,128)(2,1)S(1)}, f32[128,1024]{1,0:T(8,128)S(1)}...) custom-call(bf16[256,2048]{1,0:T(8,128)(2,1)} %tok_ref.1, ...), custom_call_target="tpu_custom_call" | custom-call | flops 17179869184 | bytes 41943040 | tf_op jit(solution)/shard_map/whole/pallas_call | solution.py:745
  159.7 3.5 %flush.1 = (bf16[2048,512]{1,0:T(8,128)(2,1)}, bf16[2048,512]{1,0:T(8,128)(2,1)}, bf16[512,2048]{1,0:T(8,128)(2,1)}, f32[128,1024]{1,0:T(8,128)}, bf16[256,2048]...) custom-call(bf16[2048,512]{1,0:T(8,128)(2,1)S(1)} %get-tuple-element.21.refs_0_, ...), custom_call_target="tpu_custom_call" | custom-call | flops 1000 | bytes 17825792 | tf_op jit(solution)/shard_map/flush/pallas_call | solution.py:694
